TPU v7x, 512 devices: a whole 4x4x16 slice. The times are simulated.
512 devices in a mesh: ep: 32 (over z, core), tp: 16 (over y, x).
Axes of the slice: x: 4, y: 4, z: 16, core: 2. Of those that a mesh axis runs over, the one named last changes fastest.
Arguments:
- queries: bfloat16 [8192, 2048], P('ep', 'tp'), may hold values from -6 to 6
- keys: bfloat16 [8192, 2048], P('ep', 'tp'), may hold values from -6 to 6
- values: bfloat16 [8192, 2048], P('ep', 'tp'), may hold values from -6 to 6
- gates: bfloat16 [8192, 2048], P('ep', 'tp'), may hold values from -6 to 6
- log_decay: float32 [8192, 16], P('ep', 'tp'), may hold values from -2 to 0
- out_weight: bfloat16 [2048, 2048], P(None, 'tp'), may hold values from -0.125 to 0.125
- moe_rows: bfloat16 [8192, 2048], P('ep'), may hold values from -140 to 140
- moe_gain: bfloat16 [2048], replicated, may hold values from 0.099609375 to 1.8984375
- routes: int32 [8192, 2], P('ep'), may hold values from 0 to 31, as said below
- route_weights: float32 [8192, 2], P('ep'), may hold values from 0.1 to 1
- gate_proj: bfloat16 [32, 2048, 4096], P('ep', None, 'tp'), may hold values from -0.125 to 0.125
- up_proj: bfloat16 [32, 2048, 4096], P('ep', None, 'tp'), may hold values from -0.125 to 0.125
- down_proj: bfloat16 [32, 4096, 2048], P('ep', None, 'tp'), may hold values from -0.09375 to 0.09375
Outputs:
- mixer_out: bfloat16 [8192, 2048], P('ep', 'tp')
- moe_out: bfloat16 [8192, 2048], P('ep', 'tp')
Inputs may be any that keep to these rules, and one draw needn't show every extreme that they name: `routes`: each row names two different experts of one group of 8 consecutive experts; in each aligned block of 256 rows every expert is named by exactly 16 rows.
All inputs are finite; a program needn't handle non-finite values.
Results may differ from a plain program's by a relative error of at most 0.011.
Values may be sent and summed in bfloat16 or wider, within the bound.
No kernel may reach another device: no remote copies, remote signals or barrier semaphores. Data moves between devices by JAX's collectives and lax.ppermute only.
A program may use at most 64 MiB of HBM per device.

v0:
```python
import jax
import jax.numpy as jnp
from jax import lax
from jax.experimental import pallas as pl
from jax.experimental.pallas import tpu as pltpu
from jax.sharding import Mesh
from jax.sharding import PartitionSpec as P

BLOCK = 128
HEAD = 128
EP = ("ep_0", "ep_1")
TP = ("tp_0", "tp_1")
BF = jnp.bfloat16
F32 = jnp.float32
HIGH = lax.Precision.HIGHEST
PAY = HEAD + 16
LIMIT = 12 * 1024 * 1024


def dot(a, b, dims=((1,), (0,)), precision=None):
    return lax.dot_general(a, b, (dims, ((), ())), precision=precision, preferred_element_type=F32)


def shaped(shape, dtype):
    return jax.ShapeDtypeStruct(shape, dtype)


def onchip(shape, dtype):
    return pltpu.VMEM(shape, dtype)


def call(body, out_shape, *args, scalars=0, far=0, scratch=()):
    near = len(args) - far
    held = [
        arg if k < scalars or k >= near else pltpu.with_memory_space_constraint(arg, pltpu.VMEM)
        for k, arg in enumerate(args)
    ]
    specs = [
        pl.BlockSpec(memory_space=pltpu.SMEM)
        if k < scalars
        else pl.BlockSpec(memory_space=pltpu.VMEM if k < near else pl.ANY)
        for k in range(len(args))
    ]
    single = not isinstance(out_shape, (list, tuple))
    outs = pl.BlockSpec(memory_space=pltpu.VMEM)
    return pl.pallas_call(
        body,
        in_specs=specs,
        out_specs=outs if single else [outs] * len(out_shape),
        out_shape=out_shape,
        scratch_shapes=list(scratch),
        compiler_params=pltpu.CompilerParams(vmem_limit_bytes=LIMIT),
    )(*held)


def route_body(turn, routes, rows, part, gain, send, slots):
    tokens = rows.shape[0]
    experts = send.shape[0]
    room = send.shape[1]
    wide = rows[...].astype(F32)
    power = jnp.mean(wide * wide, axis=-1, keepdims=True)
    normed = (part[...].astype(F32) * lax.rsqrt(power + 1e-06) * gain[...].astype(F32)).astype(BF)
    first = routes[0:1, :]
    second = routes[1:2, :]
    expert = lax.broadcasted_iota(jnp.int32, (experts, tokens), 0)
    is_first = expert == first
    is_second = expert == second
    named = jnp.where(is_first | is_second, 1.0, 0.0).astype(BF)
    earlier = lax.broadcasted_iota(jnp.int32, (tokens, tokens), 0) < lax.broadcasted_iota(
        jnp.int32, (tokens, tokens), 1
    )
    rank = dot(named, jnp.where(earlier, 1.0, 0.0).astype(BF)).astype(jnp.int32)
    slot_a = first * room + jnp.sum(jnp.where(is_first, rank, 0), axis=0, keepdims=True)
    slot_b = second * room + jnp.sum(jnp.where(is_second, rank, 0), axis=0, keepdims=True)
    slots[0:1, :] = slot_a
    slots[1:2, :] = slot_b
    place = lax.broadcasted_iota(jnp.int32, (experts * room, tokens), 0)
    chosen = jnp.where((place == slot_a) | (place == slot_b), 1.0, 0.0).astype(BF)
    send[...] = dot(chosen, normed).astype(BF).reshape(experts, room, HEAD)


def dispatch(moe_rows, moe_gain, routes, experts, turn):
    tokens, width = moe_rows.shape
    room = 2 * tokens // experts
    grid = pltpu.PrefetchScalarGridSpec(
        num_scalar_prefetch=1,
        grid=(1,),
        in_specs=[
            pl.BlockSpec((2, tokens), lambda i, t: (0, 0)),
            pl.BlockSpec((tokens, width), lambda i, t: (0, 0)),
            pl.BlockSpec((tokens, HEAD), lambda i, t: (0, t[0])),
            pl.BlockSpec((1, HEAD), lambda i, t: (0, t[0])),
        ],
        out_specs=[
            pl.BlockSpec((experts, room, HEAD), lambda i, t: (0, 0, 0)),
            pl.BlockSpec((2, tokens), lambda i, t: (0, 0)),
        ],
    )
    return pl.pallas_call(
        route_body,
        grid_spec=grid,
        out_shape=[shaped((experts, room, HEAD), BF), shaped((2, tokens), jnp.int32)],
        name="route",
        compiler_params=pltpu.CompilerParams(vmem_limit_bytes=LIMIT),
    )(turn, routes.T, moe_rows, moe_rows, moe_gain.reshape(1, width))


def spread_body(rows, out):
    flat = rows[...].reshape(out.shape[1], HEAD)
    for k in range(out.shape[0]):
        out[k] = flat


def hidden_body(rows, w_gate, w_up, out):
    parts, count, _ = rows.shape
    gate = jnp.zeros((count, w_gate.shape[2]), F32)
    up = gate
    for k in range(0, parts, 2):
        left = jnp.concatenate([rows[k], rows[k + 1]], axis=1)
        span = slice(k * HEAD, (k + 2) * HEAD)
        gate += dot(left, w_gate[0, span, :])
        up += dot(left, w_up[0, span, :])
    hidden = (gate / (1.0 + jnp.exp(-gate)) * up).astype(BF)
    for k in range(out.shape[0]):
        out[k, 0:count, :] = hidden[:, 0:HEAD]
        out[k, count:, :] = hidden[:, HEAD:]


def down_body(lane, got, w_0, w_1, w_2, w_3, out):
    peers = got.shape[0]
    count = got.shape[1] // 2
    left = [
        jnp.concatenate([got[k, 0:count, :], got[k, count:, :]], axis=1) for k in range(peers)
    ]
    for first, (one, two) in ((0, (w_0, w_1)), (2, (w_2, w_3))):
        expert = jnp.zeros((count, 2 * HEAD), F32)
        for k in range(peers):
            both = jnp.concatenate([one[k, 0 : 2 * HEAD], two[k, 0 : 2 * HEAD]], axis=1)
            expert += dot(left[k], both)
        for which in range(2):
            at = (lane[0] + peers - first - which) % peers
            cols = slice(which * HEAD, which * HEAD + HEAD)
            out[pl.ds(at, 1)] = expert[:, cols].astype(BF)[None]


def mix_body(own, h_1, h_2, h_3, w_0, w_1, w_2, w_3, row, o_0, o_1, o_2, o_3):
    peers = 4
    heads = [own[...], h_1[...], h_2[...], h_3[...]]
    for (one, two), (put, put_b) in (((w_0, w_1), (o_0, o_1)), ((w_2, w_3), (o_2, o_3))):
        mixer = jnp.zeros((own.shape[0], 2 * HEAD), F32)
        for far in range(peers):
            at = (row[0] + peers - far) % peers
            both = jnp.concatenate(
                [one[pl.ds(at, 1), 2 * HEAD :][0], two[pl.ds(at, 1), 2 * HEAD :][0]], axis=1
            )
            mixer += dot(heads[far], both)
        put[...] = mixer[:, 0:HEAD].astype(BF)
        put_b[...] = mixer[:, HEAD:].astype(BF)


def add_body(parts, out):
    total = parts[0].astype(F32)
    for k in range(1, parts.shape[0]):
        total += parts[k].astype(F32)
    out[...] = total.astype(BF).reshape(out.shape)


def add_four_body(p_0, p_1, p_2, p_3, out):
    out[...] = (
        (p_0[...].astype(F32) + p_1[...].astype(F32))
        + (p_2[...].astype(F32) + p_3[...].astype(F32))
    ).astype(BF)


def combine_body(back, slots, weights, out):
    experts, room, _ = back.shape
    rows = back[...].reshape(experts * room, HEAD)
    tokens = slots.shape[0]
    place = lax.broadcasted_iota(jnp.int32, (tokens, experts * room), 1)
    total = jnp.zeros((tokens, HEAD), F32)
    for k in range(2):
        chosen = jnp.where(place == slots[:, k : k + 1], 1.0, 0.0).astype(BF)
        total += dot(chosen, rows) * weights[:, k : k + 1]
    out[...] = total.astype(BF)


def local_body(q, k, v, decay, cosine, sine, base, q_decayed, state, pay):
    count = q.shape[0]
    blocks = count // BLOCK
    cos = cosine[...]
    sin = sine[...]
    rows = lax.broadcasted_iota(jnp.int32, (BLOCK, BLOCK), 0)
    cols = lax.broadcasted_iota(jnp.int32, (BLOCK, BLOCK), 1)
    causal = rows >= cols
    upper = jnp.where(rows <= cols, 1.0, 0.0)
    lower = jnp.where(causal, 1.0, 0.0)

    def turned(x, factor):
        wide = x.astype(F32)
        swapped = pltpu.roll(wide, HEAD // 2, 1)
        return ((wide * cos + swapped * sin) * factor).astype(BF)

    q_all = turned(q[...], 1.0)
    k_all = turned(k[...], HEAD ** (-0.5))
    carried = jnp.zeros((HEAD, HEAD), F32)
    leading = jnp.zeros((1, HEAD), F32)
    for n in range(blocks):
        span = slice(n * BLOCK, n * BLOCK + BLOCK)
        q_b, k_b, v_b = q_all[span], k_all[span], v[span, :]
        here = jnp.broadcast_to(decay[n : n + 1, :], (BLOCK, BLOCK))
        cum_i = dot(lower, here, ((1,), (1,)), HIGH)
        cum_j = dot(here, upper, precision=HIGH)
        weights = jnp.where(causal, jnp.exp(jnp.where(causal, cum_i - cum_j, 0.0)), 0.0)
        scores = dot(q_b, k_b, ((1,), (1,)))
        inside = dot((scores * weights).astype(BF), v_b)
        q_f = q_b.astype(F32)
        q_d = q_f * jnp.exp(cum_i)
        if n:
            inside += dot(q_d, carried, precision=HIGH)
        base[span, :] = inside
        q_decayed[span, :] = q_f * jnp.exp(cum_i + leading)
        ending = cum_i[BLOCK - 1 : BLOCK, :]
        k_scaled = k_b.astype(F32) * jnp.exp(ending - cum_i)
        update = dot(k_scaled, v_b.astype(F32), ((0,), (0,)), HIGH)
        carried = jnp.exp(ending) * carried + update
        leading = leading + ending
    state[0:HEAD, :] = carried
    state[HEAD:, :] = jnp.broadcast_to(leading, (8, HEAD))
    packed(pay, carried, leading)


def packed(pay, state, total):
    pay[0:HEAD, :] = state.astype(BF)
    high = total.astype(BF)
    rest = total - high.astype(F32)
    middle = rest.astype(BF)
    low = (rest - middle.astype(F32)).astype(BF)
    row = lax.broadcasted_iota(jnp.int32, (16, HEAD), 0)
    three = jnp.where(
        row == 0,
        high.astype(F32),
        jnp.where(row == 1, middle.astype(F32), jnp.where(row == 2, low.astype(F32), 0.0)),
    )
    pay[HEAD:, :] = three.astype(BF)


def unpacked(pay):
    tail = pay[HEAD:, :].astype(F32)
    return pay[0:HEAD, :].astype(F32), tail[0:1] + tail[1:2] + tail[2:3]


def pair_body(core, own, both, other, total, pay):
    state, decay = own[0:HEAD, :], own[HEAD : HEAD + 1, :]
    second = core[0] == 1
    theirs = jnp.where(second, both[0].astype(F32), both[1].astype(F32))
    other[...] = theirs.astype(BF)
    state_o = theirs[0:HEAD]
    decay_o = theirs[HEAD : HEAD + 1] + theirs[HEAD + 1 : HEAD + 2] + theirs[HEAD + 2 : HEAD + 3]
    early = jnp.where(second, state_o, state)
    late = jnp.where(second, state, state_o)
    late_decay = jnp.where(second, decay, decay_o)
    joined = late + jnp.exp(late_decay) * early
    whole = decay + decay_o
    total[0:HEAD, :] = joined
    total[HEAD:, :] = jnp.broadcast_to(whole, (8, HEAD))
    packed(pay, joined, whole)


def chain_body(before, total, got, before_out, total_out, pay):
    state, decay = unpacked(got)
    behind, behind_decay = before[0:HEAD, :], before[HEAD : HEAD + 1, :]
    before_out[0:HEAD, :] = behind + jnp.exp(behind_decay) * state
    before_out[HEAD:, :] = jnp.broadcast_to(behind_decay + decay, (8, HEAD))
    mine, mine_decay = total[0:HEAD, :], total[HEAD : HEAD + 1, :]
    joined = mine + jnp.exp(mine_decay) * state
    whole = mine_decay + decay
    total_out[0:HEAD, :] = joined
    total_out[HEAD:, :] = jnp.broadcast_to(whole, (8, HEAD))
    packed(pay, joined, whole)


def start_body(total, got, before_out, total_out, pay):
    state, decay = unpacked(got)
    before_out[0:HEAD, :] = state
    before_out[HEAD:, :] = jnp.broadcast_to(decay, (8, HEAD))
    mine, mine_decay = total[0:HEAD, :], total[HEAD : HEAD + 1, :]
    joined = mine + jnp.exp(mine_decay) * state
    whole = mine_decay + decay
    total_out[0:HEAD, :] = joined
    total_out[HEAD:, :] = jnp.broadcast_to(whole, (8, HEAD))
    packed(pay, joined, whole)


def head_body(core, base, q_decayed, before, got, other, gates, out):
    state, _ = unpacked(got)
    behind, behind_decay = before[0:HEAD, :], before[HEAD : HEAD + 1, :]
    entering = behind + jnp.exp(behind_decay) * state
    state_o, decay_o = unpacked(other)
    entering = jnp.where(core[0] == 1, state_o + jnp.exp(decay_o) * entering, entering)
    retained = base[...] + dot(q_decayed[...], entering, precision=HIGH)
    power = jnp.mean(retained * retained, axis=-1, keepdims=True)
    gate = gates[...].astype(F32)
    out[...] = (retained * lax.rsqrt(power + 1e-05) * (gate / (1.0 + jnp.exp(-gate)))).astype(BF)


def retention_heads(queries, keys, values, gates, log_decay):
    count = queries.shape[0]
    positions = (lax.axis_index(EP) * count + jnp.arange(count, dtype=jnp.int32)).astype(F32)
    half = HEAD // 2
    inverse = 10000.0 ** (-jnp.arange(half, dtype=F32) / half)
    angles = positions[:, None] * jnp.concatenate([inverse, inverse])[None, :]
    cosine = jnp.cos(angles)
    sine = jnp.sin(angles) * jnp.where(jnp.arange(HEAD) < half, -1.0, 1.0)[None, :]
    carry = onchip((HEAD + 8, HEAD), F32)
    pay_shape = onchip((PAY, HEAD), BF)
    flat = onchip((count, HEAD), F32)
    core = lax.axis_index("ep_1").reshape(1)
    base, q_decayed, own, pay = call(
        local_body,
        [flat, flat, carry, pay_shape],
        queries,
        keys,
        values,
        log_decay.reshape(count // BLOCK, BLOCK),
        cosine,
        sine,
    )
    both = lax.all_gather(pay, "ep_1")
    other, total, pay = call(pair_body, [pay_shape, carry, pay_shape], core, own, both, scalars=1)
    chips = lax.axis_size("ep_0")
    before = None
    reach = 1
    while reach < chips:
        got = lax.ppermute(pay, "ep_0", [(k, k + reach) for k in range(chips - reach)])
        if reach == 1:
            before, total, pay = call(start_body, [carry, carry, pay_shape], total, got)
        elif reach * 2 < chips:
            before, total, pay = call(chain_body, [carry, carry, pay_shape], before, total, got)
        reach *= 2
    return call(
        head_body,
        onchip((count, HEAD), BF),
        core,
        base,
        q_decayed,
        before,
        got,
        other,
        gates,
        scalars=1,
    )


def cut_body(lane, down, heads, *rest):
    peers = len(rest) - 1
    outs, sems = rest[:peers], rest[peers]
    units = down.shape[2]
    copies = []
    for far in range(peers):
        at = (lane[0] + far) % peers
        copies.append(
            pltpu.make_async_copy(down.at[:, at], outs[far].at[:, 0:units], sems.at[2 * far])
        )
        copies.append(
            pltpu.make_async_copy(heads.at[:, at], outs[far].at[:, units:], sems.at[2 * far + 1])
        )
    for copy in copies:
        copy.start()
    for copy in copies:
        copy.wait()


def shifted(array, axis, far):
    peers = lax.axis_size(axis)
    return lax.ppermute(array, axis, [(k, (k + far) % peers) for k in range(peers)])


def exchanged_weights(down_proj, out_weight, lane):
    peers = lax.axis_size("tp_1")
    rows = lax.axis_size("tp_0")
    down = down_proj.reshape(rows, peers, -1, HEAD)
    heads = out_weight.reshape(rows, peers, -1, HEAD)
    tall = down.shape[2] + heads.shape[2]
    found = call(
        cut_body,
        [onchip((rows, tall, HEAD), BF)] * peers,
        lane.reshape(1),
        down,
        heads,
        scalars=1,
        far=2,
        scratch=[pltpu.SemaphoreType.DMA((2 * peers,))],
    )
    swapped = [found[0]]
    for far in range(1, peers):
        swapped.append(shifted(found[far], "tp_1", far))
    return swapped


def both_halves(
    queries,
    keys,
    values,
    gates,
    log_decay,
    out_weight,
    moe_rows,
    moe_gain,
    routes,
    route_weights,
    gate_proj,
    up_proj,
    down_proj,
):
    experts = lax.axis_size(EP)
    members = lax.axis_size(TP)
    tokens = moe_rows.shape[0]
    positions = queries.shape[0]
    lane = lax.axis_index("tp_1")
    row = lax.axis_index("tp_0").reshape(1)
    room = 2 * tokens // experts
    count = experts * room
    rows_y = lax.axis_size("tp_0")
    peers = lax.axis_size("tp_1")
    send, slots = dispatch(moe_rows, moe_gain, routes, experts, lax.axis_index(TP).reshape(1))
    weights = exchanged_weights(down_proj, out_weight, lane)
    arrived = lax.all_to_all(send, EP, 0, 0, tiled=True)
    spread = call(spread_body, onchip((members, count, HEAD), BF), arrived)
    rows = lax.all_to_all(spread, TP, 0, 0, tiled=True)
    head_out = retention_heads(queries, keys, values, gates, log_decay)
    mixed = call(hidden_body, onchip((rows_y, 2 * count, HEAD), BF), rows, gate_proj, up_proj)
    got = lax.all_to_all(mixed, "tp_0", 0, 0, tiled=True)
    heads = [head_out]
    for far in range(1, rows_y):
        heads.append(shifted(head_out, "tp_0", far))
    partial = call(
        down_body, onchip((peers, count, HEAD), BF), lane.reshape(1), got, *weights, scalars=1
    )
    pieces = lax.all_to_all(partial, "tp_1", 0, 0, tiled=True)
    mixes = mix_call(heads, weights, row, positions)
    summed = call(add_body, onchip((experts, room, HEAD), BF), pieces)
    back = lax.all_to_all(summed, EP, 0, 0, tiled=True)
    gathered = [mixes[0]]
    for far in range(1, peers):
        gathered.append(shifted(mixes[far], "tp_1", peers - far))
    mixer_out = call(add_four_body, shaped((positions, HEAD), BF), *gathered)
    columns, scales = lax.optimization_barrier((slots.T, route_weights))
    moe_out = call(combine_body, shaped((tokens, HEAD), BF), back, columns, scales)
    return (mixer_out, moe_out)


def mix_call(heads, weights, row, positions):
    args = [*heads, *weights]
    held = [pltpu.with_memory_space_constraint(arg, pltpu.VMEM) for arg in args]
    near = pl.BlockSpec(memory_space=pltpu.VMEM)
    return pl.pallas_call(
        mix_body,
        in_specs=[near] * len(held) + [pl.BlockSpec(memory_space=pltpu.SMEM)],
        out_specs=[near] * 4,
        out_shape=[onchip((positions, HEAD), BF)] * 4,
        name="mix",
        compiler_params=pltpu.CompilerParams(vmem_limit_bytes=LIMIT),
    )(*held, row)


def solution(mesh):
    torus = Mesh(mesh.devices.reshape(16, 2, 4, 4), ("ep_0", "ep_1", "tp_0", "tp_1"))
    return jax.shard_map(
        both_halves,
        mesh=torus,
        in_specs=(
            P(EP, TP),
            P(EP, TP),
            P(EP, TP),
            P(EP, TP),
            P(EP, TP),
            P(None, TP),
            P(EP, None),
            P(),
            P(EP, None),
            P(EP, None),
            P(EP, None, TP),
            P(EP, None, TP),
            P(EP, None, TP),
        ),
        out_specs=(P(EP, TP), P(EP, TP)),
        check_vma=False,
    )
```

profile of v0, /device:TPU:6, one launch (start us, length us, event | category | flops | bytes accessed | tf_op | source)
XLA Modules:
  0.0 194.6 jit_solution(7099402533277611298)
XLA Ops:
  3.8 32.5 %all_to_all.25.rows = bf16[32,16,128]{2,1,0:T(8,128)(2,1)S(1)} all-to-all(bf16[32,16,128]{2,1,0:T(8,128)(2,1)S(1)} %get-tuple-element.52), channel_id=1, replica_groups=mesh['ep_0'=16,'ep_1'=2,'tp_0'=4,'tp_1'=4] {'ep_0','ep_1'}, dimensions={0} | all-to-all | bytes 262144 | tf_op jit(solution)/shard_map/all_to_all | solution.py:427
  36.7 32.2 %all_to_all.26.rows = bf16[16,512,128]{2,1,0:T(8,128)(2,1)S(1)} all-to-all(bf16[16,512,128]{2,1,0:T(8,128)(2,1)S(1)} %shard_map.148), channel_id=1, replica_groups=mesh['ep_0'=16,'ep_1'=2,'tp_0'=4,'tp_1'=4] {'tp_0','tp_1'}, dimensions={0} | all-to-all | bytes 4194304 | tf_op jit(solution)/shard_map/all_to_all | solution.py:429
  68.9 2.2 %shard_map.149 = bf16[4,1024,128]{2,1,0:T(8,128)(2,1)} custom-call(bf16[16,512,128]{2,1,0:T(8,128)(2,1)S(1)} %all_to_all.26.rows, bf16[1,2048,256]{2,1,0:T(8,128)(2,1)S(1)} %copy-done.1, bf16[1,2048,256]{2,1,0:T(8,128)(2,1)S(1)} %copy-done.2), custom_call_target="tpu_custom_call" | custom-call | tf_op jit(solution)/shard_map/pallas_call | solution.py:46
  71.2 3.6 %all-to-all-start.2 = ((bf16[4,1024,128]{2,1,0:T(8,128)(2,1)}), bf16[4,1024,128]{2,1,0:T(8,128)(2,1)S(1)}, u32[]{:S(2)}, u32[]{:S(2)}) async-start(bf16[4,1024,128]{2,1,0:T(8,128)(2,1)} %shard_map.149), calls=%async_computation.2 | async-start | bytes 2097152 | tf_op jit(solution)/shard_map/all_to_all | solution.py:432
  75.2 4.8 %collective-permute-start.7 = (bf16[4,384,128]{2,1,0:T(8,128)(2,1)S(1)}, bf16[4,384,128]{2,1,0:T(8,128)(2,1)S(1)}, u32[]{:S(2)}, u32[]{:S(2)}) collective-permute-start(bf16[4,384,128]{2,1,0:T(8,128)(2,1)S(1)} %get-tuple-element.45), channel_id=1, source_target_pairs={{0,1},{1,2},{2,3},{3,0},{4,5},{5,6},{6,7},{7,4},{8,9},{9,10},{10,1... | collective-permute-start | bytes 1179656 | tf_op jit(solution)/shard_map/ppermute | solution.py:375
  80.0 2.0 %collective-permute-start.8 = (bf16[4,384,128]{2,1,0:T(8,128)(2,1)S(1)}, bf16[4,384,128]{2,1,0:T(8,128)(2,1)S(1)}, u32[]{:S(2)}, u32[]{:S(2)}) collective-permute-start(bf16[4,384,128]{2,1,0:T(8,128)(2,1)S(1)} %get-tuple-element.46), channel_id=1, source_target_pairs={{0,2},{1,3},{2,0},{3,1},{4,6},{5,7},{6,4},{7,5},{8,10},{9,11},{10,... | collective-permute-start | bytes 1179656 | tf_op jit(solution)/shard_map/ppermute | solution.py:375
  82.0 3.2 %collective-permute-start.9 = (bf16[4,384,128]{2,1,0:T(8,128)(2,1)S(1)}, bf16[4,384,128]{2,1,0:T(8,128)(2,1)S(1)}, u32[]{:S(2)}, u32[]{:S(2)}) collective-permute-start(bf16[4,384,128]{2,1,0:T(8,128)(2,1)S(1)} %get-tuple-element.47), channel_id=1, source_target_pairs={{0,3},{1,0},{2,1},{3,2},{4,7},{5,4},{6,5},{7,6},{8,11},{9,8},{10,9... | collective-permute-start | bytes 1179656 | tf_op jit(solution)/shard_map/ppermute | solution.py:375
  85.3 9.6 %collective-permute-done.7.w_1 = bf16[4,384,128]{2,1,0:T(8,128)(2,1)S(1)} collective-permute-done((bf16[4,384,128]{2,1,0:T(8,128)(2,1)S(1)}, bf16[4,384,128]{2,1,0:T(8,128)(2,1)S(1)}, u32[]{:S(2)}, u32[]{:S(2)}) %collective-permute-start.7) | collective-permute-done | bytes 393248 | tf_op jit(solution)/shard_map/ppermute | solution.py:375
  95.4 5.0 %collective-permute-done.9.w_3 = bf16[4,384,128]{2,1,0:T(8,128)(2,1)S(1)} collective-permute-done((bf16[4,384,128]{2,1,0:T(8,128)(2,1)S(1)}, bf16[4,384,128]{2,1,0:T(8,128)(2,1)S(1)}, u32[]{:S(2)}, u32[]{:S(2)}) %collective-permute-start.9) | collective-permute-done | bytes 393248 | tf_op jit(solution)/shard_map/ppermute | solution.py:375
  102.0 4.6 %all-to-all-start.3 = ((bf16[4,512,128]{2,1,0:T(8,128)(2,1)}), bf16[4,512,128]{2,1,0:T(8,128)(2,1)S(1)}, u32[]{:S(2)}, u32[]{:S(2)}) async-start(bf16[4,512,128]{2,1,0:T(8,128)(2,1)} %shard_map.150), calls=%async_computation.3 | async-start | bytes 1048576 | tf_op jit(solution)/shard_map/all_to_all | solution.py:439
  106.7 7.5 %all-to-all-done.3.parts = bf16[4,512,128]{2,1,0:T(8,128)(2,1)S(1)} async-done(((bf16[4,512,128]{2,1,0:T(8,128)(2,1)}), bf16[4,512,128]{2,1,0:T(8,128)(2,1)S(1)}, u32[]{:S(2)}, u32[]{:S(2)}) %all-to-all-start.3) | async-done | bytes 524320 | tf_op jit(solution)/shard_map/all_to_all | solution.py:439
  114.9 6.3 %all-to-all-start.4 = ((bf16[32,16,128]{2,1,0:T(8,128)(2,1)}), bf16[32,16,128]{2,1,0:T(8,128)(2,1)S(1)}, u32[]{:S(2)}, u32[]{:S(2)}) async-start(bf16[32,16,128]{2,1,0:T(8,128)(2,1)} %shard_map.151), calls=%async_computation.4 | async-start | bytes 262144 | tf_op jit(solution)/shard_map/all_to_all | solution.py:442
  124.7 3.7 %collective-permute-start = (bf16[144,128]{1,0:T(8,128)(2,1)S(1)}, bf16[144,128]{1,0:T(8,128)(2,1)S(1)}, u32[]{:S(2)}, u32[]{:S(2)}) collective-permute-start(bf16[144,128]{1,0:T(8,128)(2,1)S(1)} %get-tuple-element.34), channel_id=1, source_target_pairs={{0,32},{32,64},{64,96},{96,128},{128,160},{160,192},{192,224},{224... | collective-permute-start | bytes 110600 | tf_op jit(solution)/shard_map/ppermute | solution.py:334
  130.1 5.2 %collective-permute-start.1 = (bf16[144,128]{1,0:T(8,128)(2,1)S(1)}, bf16[144,128]{1,0:T(8,128)(2,1)S(1)}, u32[]{:S(2)}, u32[]{:S(2)}) collective-permute-start(bf16[144,128]{1,0:T(8,128)(2,1)S(1)} %get-tuple-element.37), channel_id=1, source_target_pairs={{0,64},{32,96},{64,128},{96,160},{128,192},{160,224},{192,256},{22... | collective-permute-start | bytes 110600 | tf_op jit(solution)/shard_map/ppermute | solution.py:334
  137.0 10.5 %collective-permute-start.2 = (bf16[144,128]{1,0:T(8,128)(2,1)S(1)}, bf16[144,128]{1,0:T(8,128)(2,1)S(1)}, u32[]{:S(2)}, u32[]{:S(2)}) collective-permute-start(bf16[144,128]{1,0:T(8,128)(2,1)S(1)} %get-tuple-element.40), channel_id=1, source_target_pairs={{0,128},{32,160},{64,192},{96,224},{128,256},{160,288},{192,320},{... | collective-permute-start | bytes 110600 | tf_op jit(solution)/shard_map/ppermute | solution.py:334
  149.7 12.9 %collective-permute-start.3 = (bf16[144,128]{1,0:T(8,128)(2,1)S(1)}, bf16[144,128]{1,0:T(8,128)(2,1)S(1)}, u32[]{:S(2)}, u32[]{:S(2)}) collective-permute-start(bf16[144,128]{1,0:T(8,128)(2,1)S(1)} %get-tuple-element.42), channel_id=1, source_target_pairs={{0,256},{32,288},{64,320},{96,352},{128,384},{160,416},{192,448},{... | collective-permute-start | bytes 110600 | tf_op jit(solution)/shard_map/ppermute | solution.py:334
  164.6 3.6 %collective-permute-start.4 = (bf16[256,128]{1,0:T(8,128)(2,1)S(1)}, bf16[256,128]{1,0:T(8,128)(2,1)S(1)}, u32[]{:S(2)}, u32[]{:S(2)}) collective-permute-start(bf16[256,128]{1,0:T(8,128)(2,1)S(1)} %shard_map.145.own), channel_id=1, source_target_pairs={{0,4},{4,8},{8,12},{12,0},{1,5},{5,9},{9,13},{13,1},{2,6},{6,10},{... | collective-permute-start | bytes 196616 | tf_op jit(solution)/shard_map/ppermute | solution.py:375
  168.2 4.6 %collective-permute-start.5 = (bf16[256,128]{1,0:T(8,128)(2,1)S(1)}, bf16[256,128]{1,0:T(8,128)(2,1)S(1)}, u32[]{:S(2)}, u32[]{:S(2)}) collective-permute-start(bf16[256,128]{1,0:T(8,128)(2,1)S(1)} %shard_map.145.own), channel_id=1, source_target_pairs={{0,8},{4,12},{8,0},{12,4},{1,9},{5,13},{9,1},{13,5},{2,10},{6,14},... | collective-permute-start | bytes 196616 | tf_op jit(solution)/shard_map/ppermute | solution.py:375
  172.8 3.4 %collective-permute-start.6 = (bf16[256,128]{1,0:T(8,128)(2,1)S(1)}, bf16[256,128]{1,0:T(8,128)(2,1)S(1)}, u32[]{:S(2)}, u32[]{:S(2)}) collective-permute-start(bf16[256,128]{1,0:T(8,128)(2,1)S(1)} %shard_map.145.own), channel_id=1, source_target_pairs={{0,12},{4,0},{8,4},{12,8},{1,13},{5,1},{9,5},{13,9},{2,14},{6,2},{... | collective-permute-start | bytes 196616 | tf_op jit(solution)/shard_map/ppermute | solution.py:375
  176.2 2.8 %collective-permute-done.6.h_3 = bf16[256,128]{1,0:T(8,128)(2,1)S(1)} collective-permute-done((bf16[256,128]{1,0:T(8,128)(2,1)S(1)}, bf16[256,128]{1,0:T(8,128)(2,1)S(1)}, u32[]{:S(2)}, u32[]{:S(2)}) %collective-permute-start.6) | collective-permute-done | bytes 65568 | tf_op jit(solution)/shard_map/ppermute | solution.py:375
  179.4 1.9 collective-permute-start.10
  181.3 5.4 %collective-permute-start.11 = (bf16[256,128]{1,0:T(8,128)(2,1)S(1)}, bf16[256,128]{1,0:T(8,128)(2,1)S(1)}, u32[]{:S(2)}, u32[]{:S(2)}) collective-permute-start(bf16[256,128]{1,0:T(8,128)(2,1)S(1)} %get-tuple-element.50), channel_id=1, source_target_pairs={{0,2},{1,3},{2,0},{3,1},{4,6},{5,7},{6,4},{7,5},{8,10},{9,11},{10,... | collective-permute-start | bytes 196616 | tf_op jit(solution)/shard_map/ppermute | solution.py:375
  186.8 3.1 %collective-permute-start.12 = (bf16[256,128]{1,0:T(8,128)(2,1)S(1)}, bf16[256,128]{1,0:T(8,128)(2,1)S(1)}, u32[]{:S(2)}, u32[]{:S(2)}) collective-permute-start(bf16[256,128]{1,0:T(8,128)(2,1)S(1)} %get-tuple-element.51), channel_id=1, source_target_pairs={{0,1},{1,2},{2,3},{3,0},{4,5},{5,6},{6,7},{7,4},{8,9},{9,10},{10,1... | collective-permute-start | bytes 196616 | tf_op jit(solution)/shard_map/ppermute | solution.py:375
  190.2 2.8 %collective-permute-done.12.p_3 = bf16[256,128]{1,0:T(8,128)(2,1)S(1)} collective-permute-done((bf16[256,128]{1,0:T(8,128)(2,1)S(1)}, bf16[256,128]{1,0:T(8,128)(2,1)S(1)}, u32[]{:S(2)}, u32[]{:S(2)}) %collective-permute-start.12) | collective-permute-done | bytes 65568 | tf_op jit(solution)/shard_map/ppermute | solution.py:375
  (57 shorter events, 20.1 us)
Async XLA Ops:
  36.7 32.2 %copy-start.1 = (bf16[1,2048,256]{2,1,0:T(8,128)(2,1)S(1)}, bf16[1,2048,256]{2,1,0:T(8,128)(2,1)}, u32[]{:S(2)}) copy-start(bf16[1,2048,256]{2,1,0:T(8,128)(2,1)} %w_gate.1) | copy-start | bytes 3145732
  36.7 32.2 %copy-start.2 = (bf16[1,2048,256]{2,1,0:T(8,128)(2,1)S(1)}, bf16[1,2048,256]{2,1,0:T(8,128)(2,1)}, u32[]{:S(2)}) copy-start(bf16[1,2048,256]{2,1,0:T(8,128)(2,1)} %w_up.1) | copy-start | bytes 3145732
  71.2 29.3 %all-to-all-start.2 = ((bf16[4,1024,128]{2,1,0:T(8,128)(2,1)}), bf16[4,1024,128]{2,1,0:T(8,128)(2,1)S(1)}, u32[]{:S(2)}, u32[]{:S(2)}) async-start(bf16[4,1024,128]{2,1,0:T(8,128)(2,1)} %shard_map.149), calls=%async_computation.2 | async-start | bytes 2097152 | tf_op jit(solution)/shard_map/all_to_all | solution.py:432
  75.2 19.6 %collective-permute-start.7 = (bf16[4,384,128]{2,1,0:T(8,128)(2,1)S(1)}, bf16[4,384,128]{2,1,0:T(8,128)(2,1)S(1)}, u32[]{:S(2)}, u32[]{:S(2)}) collective-permute-start(bf16[4,384,128]{2,1,0:T(8,128)(2,1)S(1)} %get-tuple-element.45), channel_id=1, source_target_pairs={{0,1},{1,2},{2,3},{3,0},{4,5},{5,6},{6,7},{7,4},{8,9},{9,10},{10,1... | collective-permute-start | bytes 1179656 | tf_op jit(solution)/shard_map/ppermute | solution.py:375
  80.0 15.4 %collective-permute-start.8 = (bf16[4,384,128]{2,1,0:T(8,128)(2,1)S(1)}, bf16[4,384,128]{2,1,0:T(8,128)(2,1)S(1)}, u32[]{:S(2)}, u32[]{:S(2)}) collective-permute-start(bf16[4,384,128]{2,1,0:T(8,128)(2,1)S(1)} %get-tuple-element.46), channel_id=1, source_target_pairs={{0,2},{1,3},{2,0},{3,1},{4,6},{5,7},{6,4},{7,5},{8,10},{9,11},{10,... | collective-permute-start | bytes 1179656 | tf_op jit(solution)/shard_map/ppermute | solution.py:375
  82.0 18.4 %collective-permute-start.9 = (bf16[4,384,128]{2,1,0:T(8,128)(2,1)S(1)}, bf16[4,384,128]{2,1,0:T(8,128)(2,1)S(1)}, u32[]{:S(2)}, u32[]{:S(2)}) collective-permute-start(bf16[4,384,128]{2,1,0:T(8,128)(2,1)S(1)} %get-tuple-element.47), channel_id=1, source_target_pairs={{0,3},{1,0},{2,1},{3,2},{4,7},{5,4},{6,5},{7,6},{8,11},{9,8},{10,9... | collective-permute-start | bytes 1179656 | tf_op jit(solution)/shard_map/ppermute | solution.py:375
  100.4 21.4 %copy-start.5 = (bf16[256,128]{1,0:T(8,128)(2,1)S(1)}, bf16[256,128]{1,0:T(8,128)(2,1)}, u32[]{:S(2)}) copy-start(bf16[256,128]{1,0:T(8,128)(2,1)} %q.1) | copy-start | bytes 196612
  100.4 21.4 %copy-start.6 = (bf16[256,128]{1,0:T(8,128)(2,1)S(1)}, bf16[256,128]{1,0:T(8,128)(2,1)}, u32[]{:S(2)}) copy-start(bf16[256,128]{1,0:T(8,128)(2,1)} %k.1) | copy-start | bytes 196612
  100.4 21.4 %copy-start.7 = (bf16[256,128]{1,0:T(8,128)(2,1)S(1)}, bf16[256,128]{1,0:T(8,128)(2,1)}, u32[]{:S(2)}) copy-start(bf16[256,128]{1,0:T(8,128)(2,1)} %v.1) | copy-start | bytes 196612
  100.4 21.4 %copy-start.10 = (f32[256,1]{0,1:T(1,128)S(1)}, f32[256,1]{0,1:T(1,128)}, u32[]{:S(2)}) copy-start(f32[256,1]{0,1:T(1,128)} %param.17) | copy-start | bytes 3076
  102.0 62.3 %copy-start.8 = (bf16[256,128]{1,0:T(8,128)(2,1)S(1)}, bf16[256,128]{1,0:T(8,128)(2,1)}, u32[]{:S(2)}) copy-start(bf16[256,128]{1,0:T(8,128)(2,1)} %gates.1) | copy-start | bytes 196612
  102.0 12.2 %all-to-all-start.3 = ((bf16[4,512,128]{2,1,0:T(8,128)(2,1)}), bf16[4,512,128]{2,1,0:T(8,128)(2,1)S(1)}, u32[]{:S(2)}, u32[]{:S(2)}) async-start(bf16[4,512,128]{2,1,0:T(8,128)(2,1)} %shard_map.150), calls=%async_computation.3 | async-start | bytes 1048576 | tf_op jit(solution)/shard_map/all_to_all | solution.py:439
  114.9 75.0 %copy-start.11 = (f32[256,2]{0,1:T(2,128)S(1)}, f32[256,2]{0,1:T(2,128)}, u32[]{:S(2)}) copy-start(f32[256,2]{0,1:T(2,128)} %param.22) | copy-start | bytes 6148
  114.9 78.6 %all-to-all-start.4 = ((bf16[32,16,128]{2,1,0:T(8,128)(2,1)}), bf16[32,16,128]{2,1,0:T(8,128)(2,1)S(1)}, u32[]{:S(2)}, u32[]{:S(2)}) async-start(bf16[32,16,128]{2,1,0:T(8,128)(2,1)} %shard_map.151), calls=%async_computation.4 | async-start | bytes 262144 | tf_op jit(solution)/shard_map/all_to_all | solution.py:442
  124.7 5.3 %collective-permute-start = (bf16[144,128]{1,0:T(8,128)(2,1)S(1)}, bf16[144,128]{1,0:T(8,128)(2,1)S(1)}, u32[]{:S(2)}, u32[]{:S(2)}) collective-permute-start(bf16[144,128]{1,0:T(8,128)(2,1)S(1)} %get-tuple-element.34), channel_id=1, source_target_pairs={{0,32},{32,64},{64,96},{96,128},{128,160},{160,192},{192,224},{224... | collective-permute-start | bytes 110600 | tf_op jit(solution)/shard_map/ppermute | solution.py:334
  130.1 6.8 %collective-permute-start.1 = (bf16[144,128]{1,0:T(8,128)(2,1)S(1)}, bf16[144,128]{1,0:T(8,128)(2,1)S(1)}, u32[]{:S(2)}, u32[]{:S(2)}) collective-permute-start(bf16[144,128]{1,0:T(8,128)(2,1)S(1)} %get-tuple-element.37), channel_id=1, source_target_pairs={{0,64},{32,96},{64,128},{96,160},{128,192},{160,224},{192,256},{22... | collective-permute-start | bytes 110600 | tf_op jit(solution)/shard_map/ppermute | solution.py:334
  137.0 12.1 %collective-permute-start.2 = (bf16[144,128]{1,0:T(8,128)(2,1)S(1)}, bf16[144,128]{1,0:T(8,128)(2,1)S(1)}, u32[]{:S(2)}, u32[]{:S(2)}) collective-permute-start(bf16[144,128]{1,0:T(8,128)(2,1)S(1)} %get-tuple-element.40), channel_id=1, source_target_pairs={{0,128},{32,160},{64,192},{96,224},{128,256},{160,288},{192,320},{... | collective-permute-start | bytes 110600 | tf_op jit(solution)/shard_map/ppermute | solution.py:334
  149.7 14.6 %collective-permute-start.3 = (bf16[144,128]{1,0:T(8,128)(2,1)S(1)}, bf16[144,128]{1,0:T(8,128)(2,1)S(1)}, u32[]{:S(2)}, u32[]{:S(2)}) collective-permute-start(bf16[144,128]{1,0:T(8,128)(2,1)S(1)} %get-tuple-element.42), channel_id=1, source_target_pairs={{0,256},{32,288},{64,320},{96,352},{128,384},{160,416},{192,448},{... | collective-permute-start | bytes 110600 | tf_op jit(solution)/shard_map/ppermute | solution.py:334
  164.6 11.6 %collective-permute-start.4 = (bf16[256,128]{1,0:T(8,128)(2,1)S(1)}, bf16[256,128]{1,0:T(8,128)(2,1)S(1)}, u32[]{:S(2)}, u32[]{:S(2)}) collective-permute-start(bf16[256,128]{1,0:T(8,128)(2,1)S(1)} %shard_map.145.own), channel_id=1, source_target_pairs={{0,4},{4,8},{8,12},{12,0},{1,5},{5,9},{9,13},{13,1},{2,6},{6,10},{... | collective-permute-start | bytes 196616 | tf_op jit(solution)/shard_map/ppermute | solution.py:375
  168.2 8.0 %collective-permute-start.5 = (bf16[256,128]{1,0:T(8,128)(2,1)S(1)}, bf16[256,128]{1,0:T(8,128)(2,1)S(1)}, u32[]{:S(2)}, u32[]{:S(2)}) collective-permute-start(bf16[256,128]{1,0:T(8,128)(2,1)S(1)} %shard_map.145.own), channel_id=1, source_target_pairs={{0,8},{4,12},{8,0},{12,4},{1,9},{5,13},{9,1},{13,5},{2,10},{6,14},... | collective-permute-start | bytes 196616 | tf_op jit(solution)/shard_map/ppermute | solution.py:375
  172.8 6.2 %collective-permute-start.6 = (bf16[256,128]{1,0:T(8,128)(2,1)S(1)}, bf16[256,128]{1,0:T(8,128)(2,1)S(1)}, u32[]{:S(2)}, u32[]{:S(2)}) collective-permute-start(bf16[256,128]{1,0:T(8,128)(2,1)S(1)} %shard_map.145.own), channel_id=1, source_target_pairs={{0,12},{4,0},{8,4},{12,8},{1,13},{5,1},{9,5},{13,9},{2,14},{6,2},{... | collective-permute-start | bytes 196616 | tf_op jit(solution)/shard_map/ppermute | solution.py:375
  179.4 10.7 %collective-permute-start.10 = (bf16[256,128]{1,0:T(8,128)(2,1)S(1)}, bf16[256,128]{1,0:T(8,128)(2,1)S(1)}, u32[]{:S(2)}, u32[]{:S(2)}) collective-permute-start(bf16[256,128]{1,0:T(8,128)(2,1)S(1)} %get-tuple-element.49), channel_id=1, source_target_pairs={{0,3},{1,0},{2,1},{3,2},{4,7},{5,4},{6,5},{7,6},{8,11},{9,8},{10,9... | collective-permute-start | bytes 196616 | tf_op jit(solution)/shard_map/ppermute | solution.py:375
  181.3 8.8 %collective-permute-start.11 = (bf16[256,128]{1,0:T(8,128)(2,1)S(1)}, bf16[256,128]{1,0:T(8,128)(2,1)S(1)}, u32[]{:S(2)}, u32[]{:S(2)}) collective-permute-start(bf16[256,128]{1,0:T(8,128)(2,1)S(1)} %get-tuple-element.50), channel_id=1, source_target_pairs={{0,2},{1,3},{2,0},{3,1},{4,6},{5,7},{6,4},{7,5},{8,10},{9,11},{10,... | collective-permute-start | bytes 196616 | tf_op jit(solution)/shard_map/ppermute | solution.py:375
  186.8 6.2 %collective-permute-start.12 = (bf16[256,128]{1,0:T(8,128)(2,1)S(1)}, bf16[256,128]{1,0:T(8,128)(2,1)S(1)}, u32[]{:S(2)}, u32[]{:S(2)}) collective-permute-start(bf16[256,128]{1,0:T(8,128)(2,1)S(1)} %get-tuple-element.51), channel_id=1, source_target_pairs={{0,1},{1,2},{2,3},{3,0},{4,5},{5,6},{6,7},{7,4},{8,9},{9,10},{10,1... | collective-permute-start | bytes 196616 | tf_op jit(solution)/shard_map/ppermute | solution.py:375
  (4 other events, 9.2 us)
where the time goes:
time: 197 us; the launch traced here: 195 us
  starting transfers between devices  78.9 us (40%)
  blocking collectives  66.5 us (34%)
  waiting for transfers between devices  34.7 us (18%)
  Pallas kernels  9.91 us (5%)
  local copies, waits for them, and re-layouts  2.91 us (1%)
    all_to_all x1, blocking collectives, both_halves(): arrived = lax.all_to_all(send, EP, 0, 0, tiled=True)  32.5 us
    ppermute x4, starting transfers between devices, retention_heads(): lax.ppermute(pay, 'ep_0', [(k, k + reach) for k in range(chips - reach)])  32.3 us
    all_to_all x1, blocking collectives, both_halves(): rows = lax.all_to_all(spread, TP, 0, 0, tiled=True)  32.2 us
    ppermute x9, starting transfers between devices, shifted(): lax.ppermute(array, axis, [(k, (k + far) % peers) for k in range(peers)])  32 us
    ppermute x9, waiting for transfers between devices, shifted(): lax.ppermute(array, axis, [(k, (k + far) % peers) for k in range(peers)])  20.7 us
    pallas_call x13, Pallas kernels, call(): pl.pallas_call(body, in_specs=specs, out_specs=outs if single else [outs]...  8.94 us
    all_to_all x1, waiting for transfers between devices, both_halves(): pieces = lax.all_to_all(partial, 'tp_1', 0, 0, tiled=True)  7.5 us
    ppermute x4, waiting for transfers between devices, retention_heads(): lax.ppermute(pay, 'ep_0', [(k, k + reach) for k in range(chips - reach)])  6.47 us
  transfers between devices with their start and end apart: 16, of which 10 were waited for; matrix products, arithmetic and copies ran while one was open for 0% of the time, Pallas kernels for 2%

commit v1 on v0

v1 whole, which is shorter than its diff:
```python
import functools

import jax
import jax.numpy as jnp
from jax import lax
from jax.experimental import pallas as pl
from jax.experimental.pallas import tpu as pltpu
from jax.sharding import Mesh
from jax.sharding import PartitionSpec as P

BLOCK = 128
HEAD = 128
EP = ("ep_0", "ep_1")
TP = ("tp_0", "tp_1")
BF = jnp.bfloat16
F32 = jnp.float32
HIGH = lax.Precision.HIGHEST
PAY = HEAD + 16
LIMIT = 12 * 1024 * 1024


def dot(a, b, dims=((1,), (0,)), precision=None):
    return lax.dot_general(a, b, (dims, ((), ())), precision=precision, preferred_element_type=F32)


def shaped(shape, dtype):
    return jax.ShapeDtypeStruct(shape, dtype)


def onchip(shape, dtype):
    return pltpu.VMEM(shape, dtype)


def call(body, out_shape, *args, kinds, outs="v", scratch=()):
    places = {
        "s": pl.BlockSpec(memory_space=pltpu.SMEM),
        "v": pl.BlockSpec(memory_space=pltpu.VMEM),
        "h": pl.BlockSpec(),
        "p": pl.BlockSpec(),
        "a": pl.BlockSpec(memory_space=pltpu.HBM),
    }
    held = [
        pltpu.with_memory_space_constraint(arg, {"v": pltpu.VMEM}.get(kind, pltpu.HBM))
        if kind in "vpa"
        else arg
        for arg, kind in zip(args, kinds, strict=True)
    ]
    single = not isinstance(out_shape, (list, tuple))
    out_specs = [places[kind] for kind in outs]
    return pl.pallas_call(
        body,
        in_specs=[places[kind] for kind in kinds],
        out_specs=out_specs[0] if single else out_specs,
        out_shape=out_shape,
        scratch_shapes=list(scratch),
        compiler_params=pltpu.CompilerParams(vmem_limit_bytes=LIMIT),
    )(*held)


def route_body(turn, routes, gain, source, send, slots, rows, sems):
    tokens = rows.shape[0]
    experts = send.shape[0]
    room = send.shape[1]
    chunks = sems.shape[0]
    tall = tokens // chunks
    copies = [
        pltpu.make_async_copy(
            source.at[pl.ds(k * tall, tall)], rows.at[pl.ds(k * tall, tall)], sems.at[k]
        )
        for k in range(chunks)
    ]
    for copy in copies:
        copy.start()
    first = routes[0:1, :]
    second = routes[1:2, :]
    expert = lax.broadcasted_iota(jnp.int32, (experts, tokens), 0)
    is_first = expert == first
    is_second = expert == second
    named = jnp.where(is_first | is_second, 1.0, 0.0).astype(BF)
    earlier = lax.broadcasted_iota(jnp.int32, (tokens, tokens), 0) < lax.broadcasted_iota(
        jnp.int32, (tokens, tokens), 1
    )
    rank = dot(named, jnp.where(earlier, 1.0, 0.0).astype(BF)).astype(jnp.int32)
    slot_a = first * room + jnp.sum(jnp.where(is_first, rank, 0), axis=0, keepdims=True)
    slot_b = second * room + jnp.sum(jnp.where(is_second, rank, 0), axis=0, keepdims=True)
    slots[0:1, :] = slot_a
    slots[1:2, :] = slot_b
    place = lax.broadcasted_iota(jnp.int32, (experts * room, tokens), 0)
    chosen = jnp.where((place == slot_a) | (place == slot_b), 1.0, 0.0).astype(BF)
    which = lax.broadcasted_iota(jnp.int32, gain.shape, 0) == turn[0]
    scale = jnp.sum(jnp.where(which, gain[...].astype(F32), 0.0), axis=0, keepdims=True)
    at = pl.multiple_of(turn[0] * HEAD, HEAD)
    parts = []
    for k, copy in enumerate(copies):
        copy.wait()
        wide = rows[k * tall : (k + 1) * tall, :].astype(F32)
        power = jnp.mean(wide * wide, axis=-1, keepdims=True)
        part = rows[k * tall : (k + 1) * tall, pl.ds(at, HEAD)].astype(F32)
        parts.append((part * lax.rsqrt(power + 1e-06) * scale).astype(BF))
    normed = jnp.concatenate(parts, axis=0)
    send[...] = dot(chosen, normed).astype(BF).reshape(experts, room, HEAD)


def dispatch(moe_rows, moe_gain, routes, experts, turn):
    tokens, width = moe_rows.shape
    room = 2 * tokens // experts
    return call(
        route_body,
        [onchip((experts, room, HEAD), BF), onchip((2, tokens), jnp.int32)],
        turn,
        routes.T,
        moe_gain.reshape(width // HEAD, HEAD),
        moe_rows,
        kinds="sppa",
        outs="vv",
        scratch=[pltpu.VMEM((tokens, width), BF), pltpu.SemaphoreType.DMA((4,))],
    )


def spread_body(rows, out, sems):
    copies = [pltpu.make_async_copy(rows, out.at[k], sems.at[k]) for k in range(out.shape[0])]
    for copy in copies:
        copy.start()
    for copy in copies:
        copy.wait()


def hidden_body(rows, heads, w_gate, w_up, out, near_gate, near_up, sems):
    parts, count, _ = rows.shape
    chunks = sems.shape[1]
    tall = w_gate.shape[1] // chunks
    copies = []
    for k in range(chunks):
        span = pl.ds(k * tall, tall)
        copies.append(
            (
                pltpu.make_async_copy(w_gate.at[0, span], near_gate.at[span], sems.at[0, k]),
                pltpu.make_async_copy(w_up.at[0, span], near_up.at[span], sems.at[1, k]),
            )
        )
    for one, two in copies:
        one.start()
        two.start()
    gate = jnp.zeros((count, w_gate.shape[2]), F32)
    up = gate
    per = parts // chunks
    for k in range(chunks):
        left = jnp.concatenate([rows[k * per + j] for j in range(per)], axis=1)
        span = slice(k * tall, (k + 1) * tall)
        copies[k][0].wait()
        gate += dot(left, near_gate[span, :])
        copies[k][1].wait()
        up += dot(left, near_up[span, :])
    hidden = (gate / (1.0 + jnp.exp(-gate)) * up).astype(BF)
    for k in range(out.shape[0]):
        out[k, 0:count, :] = hidden[:, 0:HEAD]
        out[k, count : 2 * count, :] = hidden[:, HEAD:]
        out[k, 2 * count :, :] = heads[...]


def project_body(lane, got, w_0, w_1, w_2, w_3, out, n_0, n_1, n_2, n_3, sems):
    peers = got.shape[0]
    positions = got.shape[1] // 5
    count = 2 * positions
    units = 2 * HEAD
    near = (n_0, n_1, n_2, n_3)
    copies = [
        pltpu.make_async_copy(far, here, sems.at[k])
        for k, (far, here) in enumerate(zip((w_0, w_1, w_2, w_3), near, strict=True))
    ]
    for copy in copies:
        copy.start()
    left = [
        jnp.concatenate([got[k, 0:count, :], got[k, count : 2 * count, :]], axis=1)
        for k in range(peers)
    ]
    for first in (0, 2):
        one, two = near[first], near[first + 1]
        copies[first].wait()
        copies[first + 1].wait()
        expert = jnp.zeros((count, 2 * HEAD), F32)
        mixer = jnp.zeros((positions, 2 * HEAD), F32)
        for k in range(peers):
            both = jnp.concatenate([one[k], two[k]], axis=1)
            expert += dot(left[k], both[0:units])
            mixer += dot(got[k, 2 * count :, :], both[units:])
        for which in range(2):
            at = (lane[0] + peers - first - which) % peers
            cols = slice(which * HEAD, which * HEAD + HEAD)
            out[pl.ds(at, 1), 0:count, :] = expert[:, cols].astype(BF)[None]
            out[pl.ds(at, 1), count:, :] = mixer[:, cols].astype(BF)[None]


def add_body(parts, experts, mixer):
    total = parts[0].astype(F32)
    for k in range(1, parts.shape[0]):
        total += parts[k].astype(F32)
    count = experts.shape[0] * experts.shape[1]
    experts[...] = total[0:count].astype(BF).reshape(experts.shape)
    mixer[...] = total[count:].astype(BF)


def combine_body(back, slots, weights, out):
    experts, room, _ = back.shape
    rows = back[...].reshape(experts * room, HEAD)
    tokens = slots.shape[0]
    place = lax.broadcasted_iota(jnp.int32, (tokens, experts * room), 1)
    total = jnp.zeros((tokens, HEAD), F32)
    for k in range(2):
        chosen = jnp.where(place == slots[:, k : k + 1], 1.0, 0.0).astype(BF)
        total += dot(chosen, rows) * weights[:, k : k + 1]
    out[...] = total.astype(BF)


def local_body(q, k, v, decay, cosine, sine, base, q_decayed, pay):
    count = q.shape[0]
    blocks = count // BLOCK
    cos = cosine[...]
    sin = sine[...]
    rows = lax.broadcasted_iota(jnp.int32, (BLOCK, BLOCK), 0)
    cols = lax.broadcasted_iota(jnp.int32, (BLOCK, BLOCK), 1)
    causal = rows >= cols
    upper = jnp.where(rows <= cols, 1.0, 0.0)
    lower = jnp.where(causal, 1.0, 0.0)

    def turned(x, factor):
        wide = x.astype(F32)
        swapped = pltpu.roll(wide, HEAD // 2, 1)
        return ((wide * cos + swapped * sin) * factor).astype(BF)

    q_all = turned(q[...], 1.0)
    k_all = turned(k[...], HEAD ** (-0.5))
    carried = jnp.zeros((HEAD, HEAD), F32)
    leading = jnp.zeros((1, HEAD), F32)
    for n in range(blocks):
        span = slice(n * BLOCK, n * BLOCK + BLOCK)
        q_b, k_b, v_b = q_all[span], k_all[span], v[span, :]
        here = jnp.broadcast_to(decay[n : n + 1, :], (BLOCK, BLOCK))
        cum_i = dot(lower, here, ((1,), (1,)), HIGH)
        cum_j = dot(here, upper, precision=HIGH)
        weights = jnp.where(causal, jnp.exp(jnp.where(causal, cum_i - cum_j, 0.0)), 0.0)
        scores = dot(q_b, k_b, ((1,), (1,)))
        inside = dot((scores * weights).astype(BF), v_b)
        q_f = q_b.astype(F32)
        q_d = q_f * jnp.exp(cum_i)
        if n:
            inside += dot(q_d, carried, precision=HIGH)
        base[span, :] = inside
        q_decayed[span, :] = q_f * jnp.exp(cum_i + leading)
        ending = cum_i[BLOCK - 1 : BLOCK, :]
        k_scaled = k_b.astype(F32) * jnp.exp(ending - cum_i)
        update = dot(k_scaled, v_b.astype(F32), ((0,), (0,)), HIGH)
        carried = jnp.exp(ending) * carried + update
        leading = leading + ending
    packed(pay, carried, leading)


def packed(pay, state, total):
    pay[0:HEAD, :] = state.astype(BF)
    high = total.astype(BF)
    rest = total - high.astype(F32)
    middle = rest.astype(BF)
    low = (rest - middle.astype(F32)).astype(BF)
    row = lax.broadcasted_iota(jnp.int32, (16, HEAD), 0)
    three = jnp.where(
        row == 0,
        high.astype(F32),
        jnp.where(row == 1, middle.astype(F32), jnp.where(row == 2, low.astype(F32), 0.0)),
    )
    pay[HEAD:, :] = three.astype(BF)


def unpacked(pay):
    tail = pay[HEAD:, :].astype(F32)
    return pay[0:HEAD, :].astype(F32), tail[0:1] + tail[1:2] + tail[2:3]


def pair_body(both, pay):
    early, early_decay = unpacked(both.at[0])
    late, late_decay = unpacked(both.at[1])
    packed(pay, late + jnp.exp(late_decay) * early, early_decay + late_decay)


def head_body(core, chip, chips, both, base, q_decayed, gates, out):
    entering = jnp.zeros((HEAD, HEAD), F32)
    for k in range(chips.shape[0]):
        state, decay = unpacked(chips.at[k])
        entering = jnp.where(k < chip[0], jnp.exp(decay) * entering + state, entering)
    early, early_decay = unpacked(both.at[0])
    entering = jnp.where(core[0] == 1, early + jnp.exp(early_decay) * entering, entering)
    retained = base[...] + dot(q_decayed[...], entering, precision=HIGH)
    power = jnp.mean(retained * retained, axis=-1, keepdims=True)
    gate = gates[...].astype(F32)
    out[...] = (retained * lax.rsqrt(power + 1e-05) * (gate / (1.0 + jnp.exp(-gate)))).astype(BF)


def retention_heads(queries, keys, values, gates, log_decay):
    count = queries.shape[0]
    positions = (lax.axis_index(EP) * count + jnp.arange(count, dtype=jnp.int32)).astype(F32)
    half = HEAD // 2
    inverse = 10000.0 ** (-jnp.arange(half, dtype=F32) / half)
    angles = positions[:, None] * jnp.concatenate([inverse, inverse])[None, :]
    cosine = jnp.cos(angles)
    sine = jnp.sin(angles) * jnp.where(jnp.arange(HEAD) < half, -1.0, 1.0)[None, :]
    flat = shaped((count, HEAD), F32)
    base, q_decayed, pay = call(
        local_body,
        [flat, flat, onchip((PAY, HEAD), BF)],
        queries,
        keys,
        values,
        log_decay.reshape(count // BLOCK, BLOCK),
        cosine,
        sine,
        kinds="hhhhvv",
        outs="hhv",
    )
    both = lax.all_gather(pay, "ep_1")
    pay = call(pair_body, onchip((PAY, HEAD), BF), both, kinds="v")
    chips = lax.all_gather(pay, "ep_0")
    return call(
        head_body,
        shaped((count, HEAD), BF),
        lax.axis_index("ep_1").reshape(1),
        lax.axis_index("ep_0").reshape(1),
        chips,
        both,
        base,
        q_decayed,
        gates,
        kinds="sshhhhh",
        outs="h",
    )


def cut_body(far, lane, down, heads, *rest):
    peers = down.shape[1]
    outs, sems = rest[: len(far)], rest[len(far)]
    units = down.shape[2]
    copies = []
    for k, step in enumerate(far):
        at = (lane[0] + step) % peers
        copies.append(
            pltpu.make_async_copy(down.at[:, at], outs[k].at[:, 0:units], sems.at[2 * k])
        )
        copies.append(
            pltpu.make_async_copy(heads.at[:, at], outs[k].at[:, units:], sems.at[2 * k + 1])
        )
    for copy in copies:
        copy.start()
    for copy in copies:
        copy.wait()


def shifted(array, axis, far):
    peers = lax.axis_size(axis)
    return lax.ppermute(array, axis, [(k, (k + far) % peers) for k in range(peers)])


def exchanged_weights(down_proj, out_weight, lane):
    peers = lax.axis_size("tp_1")
    rows = lax.axis_size("tp_0")
    down = down_proj.reshape(rows, peers, -1, HEAD)
    heads = out_weight.reshape(rows, peers, -1, HEAD)
    shape = (rows, down.shape[2] + heads.shape[2], HEAD)

    def cut(steps, outs, places):
        return call(
            functools.partial(cut_body, steps),
            outs,
            lane.reshape(1),
            down,
            heads,
            kinds="saa",
            outs=places,
            scratch=[pltpu.SemaphoreType.DMA((2 * len(steps),))],
        )

    one, three = cut((1, 3), [onchip(shape, BF), onchip(shape, BF)], "vv")
    own, two = cut((0, 2), [pltpu.HBM(shape, BF), onchip(shape, BF)], "av")
    swapped = [own]
    for far, block in ((1, one), (2, two), (3, three)):
        swapped.append(shifted(block, "tp_1", far))
    return swapped


def both_halves(
    queries,
    keys,
    values,
    gates,
    log_decay,
    out_weight,
    moe_rows,
    moe_gain,
    routes,
    route_weights,
    gate_proj,
    up_proj,
    down_proj,
):
    experts = lax.axis_size(EP)
    members = lax.axis_size(TP)
    tokens = moe_rows.shape[0]
    positions = queries.shape[0]
    lane = lax.axis_index("tp_1")
    room = 2 * tokens // experts
    count = experts * room
    rows_y = lax.axis_size("tp_0")
    peers = lax.axis_size("tp_1")
    units = gate_proj.shape[2]
    tall = 2 * count + positions
    send, slots = dispatch(moe_rows, moe_gain, routes, experts, lax.axis_index(TP).reshape(1))
    weights = exchanged_weights(down_proj, out_weight, lane)
    arrived = lax.all_to_all(send, EP, 0, 0, tiled=True)
    spread = call(
        spread_body,
        pltpu.HBM((members, count, HEAD), BF),
        arrived.reshape(count, HEAD),
        kinds="v",
        outs="a",
        scratch=[pltpu.SemaphoreType.DMA((members,))],
    )
    rows = lax.all_to_all(spread, TP, 0, 0, tiled=True)
    head_out = retention_heads(queries, keys, values, gates, log_decay)
    width = gate_proj.shape[1]
    mixed = call(
        hidden_body,
        onchip((rows_y, tall, HEAD), BF),
        rows,
        head_out,
        gate_proj,
        up_proj,
        kinds="vhaa",
        scratch=[
            pltpu.VMEM((width, units), BF),
            pltpu.VMEM((width, units), BF),
            pltpu.SemaphoreType.DMA((2, 4)),
        ],
    )
    got = lax.all_to_all(mixed, "tp_0", 0, 0, tiled=True)
    block = pltpu.VMEM(weights[0].shape, BF)
    partial = call(
        project_body,
        onchip((peers, count + positions, HEAD), BF),
        lane.reshape(1),
        got,
        *weights,
        kinds="svaaaa",
        scratch=[block] * peers + [pltpu.SemaphoreType.DMA((peers,))],
    )
    pieces = lax.all_to_all(partial, "tp_1", 0, 0, tiled=True)
    summed, mixer_out = call(
        add_body,
        [onchip((experts, room, HEAD), BF), shaped((positions, HEAD), BF)],
        pieces,
        kinds="v",
        outs="vh",
    )
    back = lax.all_to_all(summed, EP, 0, 0, tiled=True)
    columns, scales = lax.optimization_barrier((slots.T, route_weights))
    moe_out = call(
        combine_body, shaped((tokens, HEAD), BF), back, columns, scales, kinds="vvv", outs="h"
    )
    return (mixer_out, moe_out)


def solution(mesh):
    torus = Mesh(mesh.devices.reshape(16, 2, 4, 4), ("ep_0", "ep_1", "tp_0", "tp_1"))
    return jax.shard_map(
        both_halves,
        mesh=torus,
        in_specs=(
            P(EP, TP),
            P(EP, TP),
            P(EP, TP),
            P(EP, TP),
            P(EP, TP),
            P(None, TP),
            P(EP, None),
            P(),
            P(EP, None),
            P(EP, None),
            P(EP, None, TP),
            P(EP, None, TP),
            P(EP, None, TP),
        ),
        out_specs=(P(EP, TP), P(EP, TP)),
        check_vma=False,
    )
```

time: 197 us -> 165 us (0.84)
  starting transfers between devices: 78.9 us -> 28.2 us
  Pallas kernels: 9.91 us -> 28.9 us
  blocking collectives: 66.5 us -> 75.8 us
  waiting for transfers between devices: 34.7 us -> 27.6 us
    ppermute x4 -> x0, starting transfers between devices: 32.3 us -> none  [retention_heads(): lax.ppermute(pay, 'ep_0', [(k, k + reach) for k in range(chips - reach)])]
    all_gather x0 -> x1, blocking collectives: none -> 29.4 us  [retention_heads(): chips = lax.all_gather(pay, 'ep_0')]
    ppermute x9 -> x3, starting transfers between devices: 32 us -> 8.89 us  [shifted(): lax.ppermute(array, axis, [(k, (k + far) % peers) for k in range(peers)])]
    all_to_all x1, blocking collectives: 32.2 us -> 12.1 us  [both_halves(): pieces = lax.all_to_all(partial, 'tp_1', 0, 0, tiled=True)]
    pallas_call x15 -> x11, Pallas kernels: 9.91 us -> 28.9 us  [call(): pl.pallas_call(body, in_specs=[places[kind] for kind in kinds], out_specs...]
    all_to_all x1, waiting for transfers between devices: 0.01 us -> 16.9 us  [both_halves(): back = lax.all_to_all(summed, EP, 0, 0, tiled=True)]
    ppermute x9 -> x3, waiting for transfers between devices: 20.7 us -> 10.7 us  [shifted(): lax.ppermute(array, axis, [(k, (k + far) % peers) for k in range(peers)])]
    all_to_all x1, waiting for transfers between devices: 7.5 us -> 0.01 us  [both_halves(): rows = lax.all_to_all(spread, TP, 0, 0, tiled=True)]
  transfers between devices with their start and end apart: 16 -> 6, of which waited for: 10 -> 3; matrix products, arithmetic and copies ran while one was open for 0% -> 1% of each run, Pallas kernels for 2% -> 10%
where the time goes in v1:
time: 165 us; the launch traced here: 163 us
  blocking collectives  75.8 us (46%)
  Pallas kernels  28.9 us (18%)
  starting transfers between devices  28.2 us (17%)
  waiting for transfers between devices  27.6 us (17%)
    all_to_all x1, blocking collectives, both_halves(): arrived = lax.all_to_all(send, EP, 0, 0, tiled=True)  32.5 us
    all_gather x1, blocking collectives, retention_heads(): chips = lax.all_gather(pay, 'ep_0')  29.4 us
    pallas_call x11, Pallas kernels, call(): pl.pallas_call(body, in_specs=[places[kind] for kind in kinds], out_specs...  28.9 us
    all_to_all x1, waiting for transfers between devices, both_halves(): back = lax.all_to_all(summed, EP, 0, 0, tiled=True)  16.9 us
    all_to_all x1, blocking collectives, both_halves(): pieces = lax.all_to_all(partial, 'tp_1', 0, 0, tiled=True)  12.1 us
    ppermute x3, waiting for transfers between devices, shifted(): lax.ppermute(array, axis, [(k, (k + far) % peers) for k in range(peers)])  10.7 us
    ppermute x3, starting transfers between devices, shifted(): lax.ppermute(array, axis, [(k, (k + far) % peers) for k in range(peers)])  8.89 us
    all_to_all x1, starting transfers between devices, both_halves(): rows = lax.all_to_all(spread, TP, 0, 0, tiled=True)  7.56 us
  transfers between devices with their start and end apart: 6, of which 3 were waited for; matrix products, arithmetic and copies ran while one was open for 1% of the time, Pallas kernels for 10%

profile of v1, /device:TPU:6, one launch (start us, length us, event | category | flops | bytes accessed | tf_op | source)
XLA Modules:
  0.0 163.1 jit_solution(4557802941161416915)
XLA Ops:
  0.6 2.5 %shard_map.140 = (bf16[32,16,128]{2,1,0:T(8,128)(2,1)S(1)}, s32[2,256]{1,0:T(2,128)S(1)}) custom-call(s32[1]{0:T(128)} %bitcast.1.turn, s32[2,256]{1,0:T(2,128)} %bitcast.24, bf16[16,128]{1,0:T(8,128)(2,1)} %bitcast.23, bf16[256,2048]{1,0:T(8,128)(2,1)} %source.1), custom_call_target="tpu_custom_call" | custom-call | tf_op jit(solution)/shard_map/pallas_call | solution.py:50
  3.1 32.5 %all_to_all.25 = bf16[32,16,128]{2,1,0:T(8,128)(2,1)S(1)} all-to-all(bf16[32,16,128]{2,1,0:T(8,128)(2,1)S(1)} %get-tuple-element.15), channel_id=1, replica_groups=mesh['ep_0'=16,'ep_1'=2,'tp_0'=4,'tp_1'=4] {'ep_0','ep_1'}, dimensions={0} | all-to-all | bytes 262144 | tf_op jit(solution)/shard_map/all_to_all | solution.py:415
  35.6 1.5 shard_map.141
  37.2 7.6 %all-to-all-start.1 = ((bf16[16,512,128]{2,1,0:T(8,128)(2,1)}), bf16[16,512,128]{2,1,0:T(8,128)(2,1)S(1)}, u32[]{:S(2)}, u32[]{:S(2)}) async-start(bf16[16,512,128]{2,1,0:T(8,128)(2,1)} %shard_map.141), calls=%async_computation.1 | async-start | bytes 4194304 | tf_op jit(solution)/shard_map/all_to_all | solution.py:424
  44.8 0.5 fusion
  45.4 0.9 shard_map.142
  46.4 1.9 %all-gather = bf16[288,128]{1,0:T(8,128)(2,1)S(1)} all-gather(bf16[144,128]{1,0:T(8,128)(2,1)S(1)} %get-tuple-element.16), channel_id=2, replica_groups=mesh['ep_0'=16,'ep_1'=2,'tp_0'=4,'tp_1'=4] {'ep_1'}, dimensions={0}, use_global_device_ids=true | all-gather | bytes 110592 | tf_op jit(solution)/shard_map/all_gather | solution.py:318
  48.2 29.4 %all-gather.1 = bf16[2304,128]{1,0:T(8,128)(2,1)S(1)} all-gather(bf16[144,128]{1,0:T(8,128)(2,1)S(1)} %shard_map.143), channel_id=3, replica_groups=mesh['ep_0'=16,'ep_1'=2,'tp_0'=4,'tp_1'=4] {'ep_0'}, dimensions={0}, use_global_device_ids=true | all-gather | bytes 626688 | tf_op jit(solution)/shard_map/all_gather | solution.py:320
  78.2 4.9 %shard_map.145 = bf16[4,1280,128]{2,1,0:T(8,128)(2,1)} custom-call(bf16[16,512,128]{2,1,0:T(8,128)(2,1)S(1)} %all-to-all-done.1.rows, bf16[256,128]{1,0:T(8,128)(2,1)S(1)} %shard_map.144.heads, bf16[1,2048,256]{2,1,0:T(8,128)(2,1)} %w_gate.1, bf16[1,2048,256]{2,1,0:T(8,128)(2,1)} %w_up.1), custom_call_target="tpu_custom_call" | custom-call | tf_op jit(solution)/shard_map/pallas_call | solution.py:50
  83.1 4.3 %all-to-all-start.2 = ((bf16[4,1280,128]{2,1,0:T(8,128)(2,1)}), bf16[4,1280,128]{2,1,0:T(8,128)(2,1)S(1)}, u32[]{:S(2)}, u32[]{:S(2)}) async-start(bf16[4,1280,128]{2,1,0:T(8,128)(2,1)} %shard_map.145), calls=%async_computation.2 | async-start | bytes 2621440 | tf_op jit(solution)/shard_map/all_to_all | solution.py:441
  87.4 1.2 shard_map.147
  88.5 2.6 %collective-permute-start = (bf16[4,384,128]{2,1,0:T(8,128)(2,1)S(1)}, bf16[4,384,128]{2,1,0:T(8,128)(2,1)S(1)}, u32[]{:S(2)}, u32[]{:S(2)}) collective-permute-start(bf16[4,384,128]{2,1,0:T(8,128)(2,1)S(1)} %get-tuple-element.20), channel_id=1, source_target_pairs={{0,1},{1,2},{2,3},{3,0},{4,5},{5,6},{6,7},{7,4},{8,9},{9,10},{10,1... | collective-permute-start | bytes 1179656 | tf_op jit(solution)/shard_map/ppermute | solution.py:357
  91.1 13.1 %shard_map.146 = (bf16[4,384,128]{2,1,0:T(8,128)(2,1)}, bf16[4,384,128]{2,1,0:T(8,128)(2,1)S(1)}) custom-call(s32[1]{0:T(128)} %bitcast.lane, bf16[4,4,256,128]{3,2,1,0:T(8,128)(2,1)} %bitcast.20, bf16[4,4,128,128]{3,2,1,0:T(8,128)(2,1)} %bitcast.22), custom_call_target="tpu_custom_call" | custom-call | tf_op jit(solution)/shard_map/pallas_call | solution.py:50
  104.2 4.4 %collective-permute-start.1 = (bf16[4,384,128]{2,1,0:T(8,128)(2,1)S(1)}, bf16[4,384,128]{2,1,0:T(8,128)(2,1)S(1)}, u32[]{:S(2)}, u32[]{:S(2)}) collective-permute-start(bf16[4,384,128]{2,1,0:T(8,128)(2,1)S(1)} %get-tuple-element.21), channel_id=1, source_target_pairs={{0,2},{1,3},{2,0},{3,1},{4,6},{5,7},{6,4},{7,5},{8,10},{9,11},{10,... | collective-permute-start | bytes 1179656 | tf_op jit(solution)/shard_map/ppermute | solution.py:357
  108.6 1.9 %collective-permute-start.2 = (bf16[4,384,128]{2,1,0:T(8,128)(2,1)S(1)}, bf16[4,384,128]{2,1,0:T(8,128)(2,1)S(1)}, u32[]{:S(2)}, u32[]{:S(2)}) collective-permute-start(bf16[4,384,128]{2,1,0:T(8,128)(2,1)S(1)} %get-tuple-element.22), channel_id=1, source_target_pairs={{0,3},{1,0},{2,1},{3,2},{4,7},{5,4},{6,5},{7,6},{8,11},{9,8},{10,9... | collective-permute-start | bytes 1179656 | tf_op jit(solution)/shard_map/ppermute | solution.py:357
  110.5 6.6 %collective-permute-done.1.w_2 = bf16[4,384,128]{2,1,0:T(8,128)(2,1)S(1)} collective-permute-done((bf16[4,384,128]{2,1,0:T(8,128)(2,1)S(1)}, bf16[4,384,128]{2,1,0:T(8,128)(2,1)S(1)}, u32[]{:S(2)}, u32[]{:S(2)}) %collective-permute-start.1) | collective-permute-done | bytes 393248 | tf_op jit(solution)/shard_map/ppermute | solution.py:357
  117.2 4.1 %collective-permute-done.2.w_3 = bf16[4,384,128]{2,1,0:T(8,128)(2,1)S(1)} collective-permute-done((bf16[4,384,128]{2,1,0:T(8,128)(2,1)S(1)}, bf16[4,384,128]{2,1,0:T(8,128)(2,1)S(1)}, u32[]{:S(2)}, u32[]{:S(2)}) %collective-permute-start.2) | collective-permute-done | bytes 393248 | tf_op jit(solution)/shard_map/ppermute | solution.py:357
  121.3 0.7 copy-done.7
  122.0 2.6 %shard_map.148 = bf16[4,768,128]{2,1,0:T(8,128)(2,1)S(1)} custom-call(s32[1]{0:T(128)} %bitcast.lane, bf16[4,1280,128]{2,1,0:T(8,128)(2,1)S(1)} %all-to-all-done.2.got, bf16[4,384,128]{2,1,0:T(8,128)(2,1)} %get-tuple-element.19.w_0, bf16[4,384,128]{2,1,0:T(8,128)(2,1)} %copy-done.5, bf16[4,384,128]{2,1,0:T(8,128)(2,1)} %copy-done.6, ...), custom_call_target="tpu_custom_call" | custom-call | tf_op jit(solution)/shard_map/pallas_call | solution.py:50
  124.6 12.1 %all_to_all.26.parts = bf16[4,768,128]{2,1,0:T(8,128)(2,1)S(1)} all-to-all(bf16[4,768,128]{2,1,0:T(8,128)(2,1)S(1)} %shard_map.148), channel_id=1, replica_groups=mesh['ep_0'=16,'ep_1'=2,'tp_0'=4,'tp_1'=4] {'tp_1'}, dimensions={0} | all-to-all | bytes 1572864 | tf_op jit(solution)/shard_map/all_to_all | solution.py:452
  136.7 0.7 shard_map.149
  137.5 7.5 %all-to-all-start.4 = ((bf16[32,16,128]{2,1,0:T(8,128)(2,1)}), bf16[32,16,128]{2,1,0:T(8,128)(2,1)S(1)}, u32[]{:S(2)}, u32[]{:S(2)}) async-start(bf16[32,16,128]{2,1,0:T(8,128)(2,1)} %get-tuple-element.24), calls=%async_computation.4 | async-start | bytes 262144 | tf_op jit(solution)/shard_map/all_to_all | solution.py:460
  145.2 16.9 %all-to-all-done.4.back = bf16[32,16,128]{2,1,0:T(8,128)(2,1)S(1)} async-done(((bf16[32,16,128]{2,1,0:T(8,128)(2,1)}), bf16[32,16,128]{2,1,0:T(8,128)(2,1)S(1)}, u32[]{:S(2)}, u32[]{:S(2)}) %all-to-all-start.4) | async-done | bytes 131104 | tf_op jit(solution)/shard_map/all_to_all | solution.py:460
  162.1 1.0 shard_map.150
  (27 shorter events, 1.0 us)
Async XLA Ops:
  37.1 8.3 %copy-start = (bf16[256,128]{1,0:T(8,128)(2,1)S(1)}, bf16[256,128]{1,0:T(8,128)(2,1)}, u32[]{:S(2)}) copy-start(bf16[256,128]{1,0:T(8,128)(2,1)} %q.1) | copy-start | bytes 196612
  37.1 8.3 %copy-start.1 = (bf16[256,128]{1,0:T(8,128)(2,1)S(1)}, bf16[256,128]{1,0:T(8,128)(2,1)}, u32[]{:S(2)}) copy-start(bf16[256,128]{1,0:T(8,128)(2,1)} %k.1) | copy-start | bytes 196612
  37.1 8.3 %copy-start.2 = (bf16[256,128]{1,0:T(8,128)(2,1)S(1)}, bf16[256,128]{1,0:T(8,128)(2,1)}, u32[]{:S(2)}) copy-start(bf16[256,128]{1,0:T(8,128)(2,1)} %v.1) | copy-start | bytes 196612
  37.1 8.3 %copy-start.4 = (f32[256,1]{0,1:T(1,128)S(1)}, f32[256,1]{0,1:T(1,128)}, u32[]{:S(2)}) copy-start(f32[256,1]{0,1:T(1,128)} %param.17) | copy-start | bytes 3076
  37.2 40.5 %copy-start.3 = (bf16[256,128]{1,0:T(8,128)(2,1)S(1)}, bf16[256,128]{1,0:T(8,128)(2,1)}, u32[]{:S(2)}) copy-start(bf16[256,128]{1,0:T(8,128)(2,1)} %gates.1) | copy-start | bytes 196612
  37.2 41.0 %all-to-all-start.1 = ((bf16[16,512,128]{2,1,0:T(8,128)(2,1)}), bf16[16,512,128]{2,1,0:T(8,128)(2,1)S(1)}, u32[]{:S(2)}, u32[]{:S(2)}) async-start(bf16[16,512,128]{2,1,0:T(8,128)(2,1)} %shard_map.141), calls=%async_computation.1 | async-start | bytes 4194304 | tf_op jit(solution)/shard_map/all_to_all | solution.py:424
  83.1 38.2 %all-to-all-start.2 = ((bf16[4,1280,128]{2,1,0:T(8,128)(2,1)}), bf16[4,1280,128]{2,1,0:T(8,128)(2,1)S(1)}, u32[]{:S(2)}, u32[]{:S(2)}) async-start(bf16[4,1280,128]{2,1,0:T(8,128)(2,1)} %shard_map.145), calls=%async_computation.2 | async-start | bytes 2621440 | tf_op jit(solution)/shard_map/all_to_all | solution.py:441
  88.5 22.0 %collective-permute-start = (bf16[4,384,128]{2,1,0:T(8,128)(2,1)S(1)}, bf16[4,384,128]{2,1,0:T(8,128)(2,1)S(1)}, u32[]{:S(2)}, u32[]{:S(2)}) collective-permute-start(bf16[4,384,128]{2,1,0:T(8,128)(2,1)S(1)} %get-tuple-element.20), channel_id=1, source_target_pairs={{0,1},{1,2},{2,3},{3,0},{4,5},{5,6},{6,7},{7,4},{8,9},{9,10},{10,1... | collective-permute-start | bytes 1179656 | tf_op jit(solution)/shard_map/ppermute | solution.py:357
  104.2 13.0 %collective-permute-start.1 = (bf16[4,384,128]{2,1,0:T(8,128)(2,1)S(1)}, bf16[4,384,128]{2,1,0:T(8,128)(2,1)S(1)}, u32[]{:S(2)}, u32[]{:S(2)}) collective-permute-start(bf16[4,384,128]{2,1,0:T(8,128)(2,1)S(1)} %get-tuple-element.21), channel_id=1, source_target_pairs={{0,2},{1,3},{2,0},{3,1},{4,6},{5,7},{6,4},{7,5},{8,10},{9,11},{10,... | collective-permute-start | bytes 1179656 | tf_op jit(solution)/shard_map/ppermute | solution.py:357
  108.6 12.7 %collective-permute-start.2 = (bf16[4,384,128]{2,1,0:T(8,128)(2,1)S(1)}, bf16[4,384,128]{2,1,0:T(8,128)(2,1)S(1)}, u32[]{:S(2)}, u32[]{:S(2)}) collective-permute-start(bf16[4,384,128]{2,1,0:T(8,128)(2,1)S(1)} %get-tuple-element.22), channel_id=1, source_target_pairs={{0,3},{1,0},{2,1},{3,2},{4,7},{5,4},{6,5},{7,6},{8,11},{9,8},{10,9... | collective-permute-start | bytes 1179656 | tf_op jit(solution)/shard_map/ppermute | solution.py:357
  110.5 10.8 %copy-start.5 = (bf16[4,384,128]{2,1,0:T(8,128)(2,1)}, bf16[4,384,128]{2,1,0:T(8,128)(2,1)S(1)}, u32[]{:S(2)}) copy-start(bf16[4,384,128]{2,1,0:T(8,128)(2,1)S(1)} %collective-permute-done.w_1) | copy-start | bytes 1179652
  117.1 4.1 %copy-start.6 = (bf16[4,384,128]{2,1,0:T(8,128)(2,1)}, bf16[4,384,128]{2,1,0:T(8,128)(2,1)S(1)}, u32[]{:S(2)}) copy-start(bf16[4,384,128]{2,1,0:T(8,128)(2,1)S(1)} %collective-permute-done.1.w_2) | copy-start | bytes 1179652
  121.3 0.7 copy-start.7
  124.6 20.5 %copy-start.8 = (f32[256,2]{0,1:T(2,128)S(1)}, f32[256,2]{0,1:T(2,128)}, u32[]{:S(2)}) copy-start(f32[256,2]{0,1:T(2,128)} %param.22) | copy-start | bytes 6148
  137.5 24.7 %all-to-all-start.4 = ((bf16[32,16,128]{2,1,0:T(8,128)(2,1)}), bf16[32,16,128]{2,1,0:T(8,128)(2,1)S(1)}, u32[]{:S(2)}, u32[]{:S(2)}) async-start(bf16[32,16,128]{2,1,0:T(8,128)(2,1)} %get-tuple-element.24), calls=%async_computation.4 | async-start | bytes 262144 | tf_op jit(solution)/shard_map/all_to_all | solution.py:460

commit v2 on v1

--- a/solution.py
+++ b/solution.py
@@ -10,7 +10,7 @@
 
 BLOCK = 128
 HEAD = 128
-EP = ("ep_0", "ep_1")
+EP = ("ep_0", "ep_1", "ep_2")
 TP = ("tp_0", "tp_1")
 BF = jnp.bfloat16
 F32 = jnp.float32
@@ -57,7 +57,7 @@
     )(*held)
 
 
-def route_body(turn, routes, gain, source, send, slots, rows, sems):
+def route_body(turn, routes_far, gain_far, source, send, slots, routes, gain, rows, sems, extra):
     tokens = rows.shape[0]
     experts = send.shape[0]
     room = send.shape[1]
@@ -69,8 +69,13 @@
         )
         for k in range(chunks)
     ]
+    small = pltpu.make_async_copy(routes_far, routes, extra.at[0])
+    scales = pltpu.make_async_copy(gain_far, gain, extra.at[1])
+    small.start()
     for copy in copies:
         copy.start()
+    scales.start()
+    small.wait()
     first = routes[0:1, :]
     second = routes[1:2, :]
     expert = lax.broadcasted_iota(jnp.int32, (experts, tokens), 0)
@@ -87,6 +92,7 @@
     slots[1:2, :] = slot_b
     place = lax.broadcasted_iota(jnp.int32, (experts * room, tokens), 0)
     chosen = jnp.where((place == slot_a) | (place == slot_b), 1.0, 0.0).astype(BF)
+    scales.wait()
     which = lax.broadcasted_iota(jnp.int32, gain.shape, 0) == turn[0]
     scale = jnp.sum(jnp.where(which, gain[...].astype(F32), 0.0), axis=0, keepdims=True)
     at = pl.multiple_of(turn[0] * HEAD, HEAD)
@@ -111,9 +117,15 @@
         routes.T,
         moe_gain.reshape(width // HEAD, HEAD),
         moe_rows,
-        kinds="sppa",
+        kinds="saaa",
         outs="vv",
-        scratch=[pltpu.VMEM((tokens, width), BF), pltpu.SemaphoreType.DMA((4,))],
+        scratch=[
+            pltpu.VMEM((2, tokens), jnp.int32),
+            pltpu.VMEM((width // HEAD, HEAD), BF),
+            pltpu.VMEM((tokens, width), BF),
+            pltpu.SemaphoreType.DMA((8,)),
+            pltpu.SemaphoreType.DMA((2,)),
+        ],
     )
 
 
@@ -125,8 +137,9 @@
         copy.wait()
 
 
-def hidden_body(rows, heads, w_gate, w_up, out, near_gate, near_up, sems):
+def hidden_body(rows, heads, w_gate, w_up, out, near_gate, near_up, near, sems, ends):
     parts, count, _ = rows.shape
+    copied = out.shape[0]
     chunks = sems.shape[1]
     tall = w_gate.shape[1] // chunks
     copies = []
@@ -141,6 +154,7 @@
     for one, two in copies:
         one.start()
         two.start()
+    near[2 * count :, :] = heads[...]
     gate = jnp.zeros((count, w_gate.shape[2]), F32)
     up = gate
     per = parts // chunks
@@ -152,32 +166,27 @@
         copies[k][1].wait()
         up += dot(left, near_up[span, :])
     hidden = (gate / (1.0 + jnp.exp(-gate)) * up).astype(BF)
-    for k in range(out.shape[0]):
-        out[k, 0:count, :] = hidden[:, 0:HEAD]
-        out[k, count : 2 * count, :] = hidden[:, HEAD:]
-        out[k, 2 * count :, :] = heads[...]
-
-
-def project_body(lane, got, w_0, w_1, w_2, w_3, out, n_0, n_1, n_2, n_3, sems):
+    near[0:count, :] = hidden[:, 0:HEAD]
+    near[count : 2 * count, :] = hidden[:, HEAD:]
+    final = [pltpu.make_async_copy(near, out.at[k], ends.at[k]) for k in range(copied)]
+    for copy in final:
+        copy.start()
+    for copy in final:
+        copy.wait()
+
+
+def project_body(lane, got, w_0, w_1, w_2, w_3, out):
     peers = got.shape[0]
     positions = got.shape[1] // 5
     count = 2 * positions
     units = 2 * HEAD
-    near = (n_0, n_1, n_2, n_3)
-    copies = [
-        pltpu.make_async_copy(far, here, sems.at[k])
-        for k, (far, here) in enumerate(zip((w_0, w_1, w_2, w_3), near, strict=True))
-    ]
-    for copy in copies:
-        copy.start()
+    near = (w_0, w_1, w_2, w_3)
     left = [
         jnp.concatenate([got[k, 0:count, :], got[k, count : 2 * count, :]], axis=1)
         for k in range(peers)
     ]
     for first in (0, 2):
         one, two = near[first], near[first + 1]
-        copies[first].wait()
-        copies[first + 1].wait()
         expert = jnp.zeros((count, 2 * HEAD), F32)
         mixer = jnp.zeros((positions, 2 * HEAD), F32)
         for k in range(peers):
@@ -256,7 +265,7 @@
 
 
 def packed(pay, state, total):
-    pay[0:HEAD, :] = state.astype(BF)
+    pay[0 : state.shape[0], :] = state.astype(BF)
     high = total.astype(BF)
     rest = total - high.astype(F32)
     middle = rest.astype(BF)
@@ -267,27 +276,36 @@
         high.astype(F32),
         jnp.where(row == 1, middle.astype(F32), jnp.where(row == 2, low.astype(F32), 0.0)),
     )
-    pay[HEAD:, :] = three.astype(BF)
+    pay[state.shape[0] :, :] = three.astype(BF)
 
 
 def unpacked(pay):
-    tail = pay[HEAD:, :].astype(F32)
-    return pay[0:HEAD, :].astype(F32), tail[0:1] + tail[1:2] + tail[2:3]
-
-
-def pair_body(both, pay):
-    early, early_decay = unpacked(both.at[0])
-    late, late_decay = unpacked(both.at[1])
-    packed(pay, late + jnp.exp(late_decay) * early, early_decay + late_decay)
-
-
-def head_body(core, chip, chips, both, base, q_decayed, gates, out):
+    rows = pay.shape[0] - 16
+    tail = pay[rows:, :].astype(F32)
+    return pay[0:rows, :].astype(F32), tail[0:1] + tail[1:2] + tail[2:3]
+
+
+def quad_body(core, near, pay):
+    state, decay = unpacked(near.at[0])
+    for k in range(1, near.shape[0]):
+        later, later_decay = unpacked(near.at[k])
+        state = later + jnp.exp(later_decay) * state
+        decay = decay + later_decay
+    half = HEAD // 2
+    mine = jnp.where(core[0] == 0, state[0:half], state[half:])
+    packed(pay, mine, decay)
+
+
+def head_body(place, group, far, near, base, q_decayed, gates, out):
     entering = jnp.zeros((HEAD, HEAD), F32)
-    for k in range(chips.shape[0]):
-        state, decay = unpacked(chips.at[k])
-        entering = jnp.where(k < chip[0], jnp.exp(decay) * entering + state, entering)
-    early, early_decay = unpacked(both.at[0])
-    entering = jnp.where(core[0] == 1, early + jnp.exp(early_decay) * entering, entering)
+    for k in range(far.shape[0] // 2):
+        upper, decay = unpacked(far.at[2 * k])
+        lower, _ = unpacked(far.at[2 * k + 1])
+        state = jnp.concatenate([upper, lower], axis=0)
+        entering = jnp.where(k < group[0], jnp.exp(decay) * entering + state, entering)
+    for k in range(near.shape[0] - 1):
+        state, decay = unpacked(near.at[k])
+        entering = jnp.where(k < place[0], jnp.exp(decay) * entering + state, entering)
     retained = base[...] + dot(q_decayed[...], entering, precision=HIGH)
     power = jnp.mean(retained * retained, axis=-1, keepdims=True)
     gate = gates[...].astype(F32)
@@ -302,7 +320,7 @@
     angles = positions[:, None] * jnp.concatenate([inverse, inverse])[None, :]
     cosine = jnp.cos(angles)
     sine = jnp.sin(angles) * jnp.where(jnp.arange(HEAD) < half, -1.0, 1.0)[None, :]
-    flat = shaped((count, HEAD), F32)
+    flat = pltpu.HBM((count, HEAD), F32)
     base, q_decayed, pay = call(
         local_body,
         [flat, flat, onchip((PAY, HEAD), BF)],
@@ -315,20 +333,27 @@
         kinds="hhhhvv",
         outs="hhv",
     )
-    both = lax.all_gather(pay, "ep_1")
-    pay = call(pair_body, onchip((PAY, HEAD), BF), both, kinds="v")
-    chips = lax.all_gather(pay, "ep_0")
+    place = lax.axis_index(("ep_1", "ep_2")).reshape(1)
+    near = lax.all_gather(pay, ("ep_1", "ep_2"))
+    pay = call(
+        quad_body,
+        onchip((PAY - HEAD // 2, HEAD), BF),
+        lax.axis_index("ep_2").reshape(1),
+        near,
+        kinds="sv",
+    )
+    far = lax.all_gather(pay, ("ep_0", "ep_2"))
     return call(
         head_body,
         shaped((count, HEAD), BF),
-        lax.axis_index("ep_1").reshape(1),
+        place,
         lax.axis_index("ep_0").reshape(1),
-        chips,
-        both,
+        far,
+        near,
         base,
         q_decayed,
         gates,
-        kinds="sshhhhh",
+        kinds="sshhpph",
         outs="h",
     )
 
@@ -376,8 +401,8 @@
             scratch=[pltpu.SemaphoreType.DMA((2 * len(steps),))],
         )
 
-    one, three = cut((1, 3), [onchip(shape, BF), onchip(shape, BF)], "vv")
-    own, two = cut((0, 2), [pltpu.HBM(shape, BF), onchip(shape, BF)], "av")
+    place = pltpu.HBM(shape, BF)
+    one, three, own, two = cut((1, 3, 0, 2), [place] * peers, "aaaa")
     swapped = [own]
     for far, block in ((1, one), (2, two), (3, three)):
         swapped.append(shifted(block, "tp_1", far))
@@ -426,28 +451,29 @@
     width = gate_proj.shape[1]
     mixed = call(
         hidden_body,
-        onchip((rows_y, tall, HEAD), BF),
+        pltpu.HBM((rows_y, tall, HEAD), BF),
         rows,
         head_out,
         gate_proj,
         up_proj,
-        kinds="vhaa",
+        kinds="vvaa",
+        outs="a",
         scratch=[
             pltpu.VMEM((width, units), BF),
             pltpu.VMEM((width, units), BF),
-            pltpu.SemaphoreType.DMA((2, 4)),
+            pltpu.VMEM((tall, HEAD), BF),
+            pltpu.SemaphoreType.DMA((2, 8)),
+            pltpu.SemaphoreType.DMA((rows_y,)),
         ],
     )
     got = lax.all_to_all(mixed, "tp_0", 0, 0, tiled=True)
-    block = pltpu.VMEM(weights[0].shape, BF)
     partial = call(
         project_body,
         onchip((peers, count + positions, HEAD), BF),
         lane.reshape(1),
         got,
         *weights,
-        kinds="svaaaa",
-        scratch=[block] * peers + [pltpu.SemaphoreType.DMA((peers,))],
+        kinds="svhhhh",
     )
     pieces = lax.all_to_all(partial, "tp_1", 0, 0, tiled=True)
     summed, mixer_out = call(
@@ -466,7 +492,7 @@
 
 
 def solution(mesh):
-    torus = Mesh(mesh.devices.reshape(16, 2, 4, 4), ("ep_0", "ep_1", "tp_0", "tp_1"))
+    torus = Mesh(mesh.devices.reshape(8, 2, 2, 4, 4), ("ep_0", "ep_1", "ep_2", "tp_0", "tp_1"))
     return jax.shard_map(
         both_halves,
         mesh=torus,

time: 165 us -> 201 us (1.22)
  Pallas kernels: 28.9 us -> 63.9 us
  waiting for transfers between devices: 27.6 us -> 33.3 us
  blocking collectives: 75.8 us -> 70.4 us
    pallas_call x11 -> x10, Pallas kernels: 28.9 us -> 63.9 us  [call(): pl.pallas_call(body, in_specs=[places[kind] for kind in kinds], out_specs...]
    all_gather x2, blocking collectives: 31.2 us -> 23.2 us  [the longest x1 17.8 us: retention_heads(): far = lax.all_gather(pay, ('ep_0', 'ep_2'))]
    ppermute x3, waiting for transfers between devices: 10.7 us -> 16.4 us  [shifted(): lax.ppermute(array, axis, [(k, (k + far) % peers) for k in range(peers)])]
    all_to_all x1, blocking collectives: 12.1 us -> 14.7 us  [both_halves(): pieces = lax.all_to_all(partial, 'tp_1', 0, 0, tiled=True)]
  transfers between devices with their start and end apart: 6 -> 6, of which waited for: 3 -> 4; matrix products, arithmetic and copies ran while one was open for 1% -> 0% of each run, Pallas kernels for 10% -> 26%
where the time goes in v2:
time: 201 us; the launch traced here: 199 us
  blocking collectives  70.4 us (35%)
  Pallas kernels  63.9 us (32%)
  waiting for transfers between devices  33.3 us (17%)
  starting transfers between devices  28.8 us (14%)
    pallas_call x10, Pallas kernels, call(): pl.pallas_call(body, in_specs=[places[kind] for kind in kinds], out_specs...  63.9 us
    all_to_all x1, blocking collectives, both_halves(): arrived = lax.all_to_all(send, EP, 0, 0, tiled=True)  32.5 us
    all_gather x1, blocking collectives, retention_heads(): far = lax.all_gather(pay, ('ep_0', 'ep_2'))  17.8 us
    all_to_all x1, waiting for transfers between devices, both_halves(): back = lax.all_to_all(summed, EP, 0, 0, tiled=True)  16.9 us
    ppermute x3, waiting for transfers between devices, shifted(): lax.ppermute(array, axis, [(k, (k + far) % peers) for k in range(peers)])  16.4 us
    all_to_all x1, blocking collectives, both_halves(): pieces = lax.all_to_all(partial, 'tp_1', 0, 0, tiled=True)  14.7 us
    ppermute x3, starting transfers between devices, shifted(): lax.ppermute(array, axis, [(k, (k + far) % peers) for k in range(peers)])  8.88 us
    all_to_all x1, starting transfers between devices, both_halves(): back = lax.all_to_all(summed, EP, 0, 0, tiled=True)  8.1 us
  transfers between devices with their start and end apart: 6, of which 4 were waited for; matrix products, arithmetic and copies ran while one was open for 0% of the time, Pallas kernels for 26%

profile of v2, /device:TPU:6, one launch (start us, length us, event | category | flops | bytes accessed | tf_op | source)
XLA Modules:
  0.0 199.2 jit_solution(2579240754568758693)
XLA Ops:
  0.6 2.6 %shard_map.140 = (bf16[32,16,128]{2,1,0:T(8,128)(2,1)S(1)}, s32[2,256]{1,0:T(2,128)S(1)}) custom-call(s32[1]{0:T(128)} %bitcast.1.turn, s32[2,256]{1,0:T(2,128)} %bitcast.23, bf16[16,128]{1,0:T(8,128)(2,1)} %bitcast.22, bf16[256,2048]{1,0:T(8,128)(2,1)} %source.1), custom_call_target="tpu_custom_call" | custom-call | tf_op jit(solution)/shard_map/pallas_call | solution.py:50
  3.2 32.5 %all_to_all.25 = bf16[32,16,128]{2,1,0:T(8,128)(2,1)S(1)} all-to-all(bf16[32,16,128]{2,1,0:T(8,128)(2,1)S(1)} %get-tuple-element.15), channel_id=1, replica_groups=mesh['ep_0'=8,'ep_1'=2,'ep_2'=2,'tp_0'=4,'tp_1'=4] {'ep_0','ep_1','ep_2'}, dimensions={0} | all-to-all | bytes 262144 | tf_op jit(solution)/shard_map/all_to_all | solution.py:440
  35.7 1.5 shard_map.141
  37.2 7.6 %all-to-all-start.1 = ((bf16[16,512,128]{2,1,0:T(8,128)(2,1)}), bf16[16,512,128]{2,1,0:T(8,128)(2,1)S(1)}, u32[]{:S(2)}, u32[]{:S(2)}) async-start(bf16[16,512,128]{2,1,0:T(8,128)(2,1)} %shard_map.141), calls=%async_computation.1 | async-start | bytes 4194304 | tf_op jit(solution)/shard_map/all_to_all | solution.py:449
  45.5 1.6 shard_map.142
  47.1 5.4 %all-gather = bf16[576,128]{1,0:T(8,128)(2,1)S(1)} all-gather(bf16[144,128]{1,0:T(8,128)(2,1)S(1)} %get-tuple-element.16), channel_id=2, replica_groups=mesh['ep_0'=8,'ep_1'=2,'ep_2'=2,'tp_0'=4,'tp_1'=4] {'ep_1','ep_2'}, dimensions={0}, use_global_device_ids=true | all-gather | bytes 184320 | tf_op jit(solution)/shard_map/all_gather | solution.py:337
  52.6 17.8 %all-gather.1 = bf16[1280,128]{1,0:T(8,128)(2,1)S(1)} all-gather(bf16[80,128]{1,0:T(8,128)(2,1)S(1)} %shard_map.143), channel_id=3, replica_groups=mesh['ep_0'=8,'ep_1'=2,'ep_2'=2,'tp_0'=4,'tp_1'=4] {'ep_0','ep_2'}, dimensions={0}, use_global_device_ids=true | all-gather | bytes 348160 | tf_op jit(solution)/shard_map/all_gather | solution.py:345
  70.3 1.4 shard_map.144.heads
  71.8 5.3 %shard_map.145 = bf16[4,1280,128]{2,1,0:T(8,128)(2,1)} custom-call(bf16[16,512,128]{2,1,0:T(8,128)(2,1)S(1)} %all-to-all-done.1.rows, bf16[256,128]{1,0:T(8,128)(2,1)S(1)} %shard_map.144.heads, bf16[1,2048,256]{2,1,0:T(8,128)(2,1)} %w_gate.1, bf16[1,2048,256]{2,1,0:T(8,128)(2,1)} %w_up.1), custom_call_target="tpu_custom_call" | custom-call | tf_op jit(solution)/shard_map/pallas_call | solution.py:50
  77.0 4.2 %all-to-all-start.2 = ((bf16[4,1280,128]{2,1,0:T(8,128)(2,1)}), bf16[4,1280,128]{2,1,0:T(8,128)(2,1)S(1)}, u32[]{:S(2)}, u32[]{:S(2)}) async-start(bf16[4,1280,128]{2,1,0:T(8,128)(2,1)} %shard_map.145), calls=%async_computation.2 | async-start | bytes 2621440 | tf_op jit(solution)/shard_map/all_to_all | solution.py:469
  81.3 48.8 %shard_map.146 = (bf16[4,384,128]{2,1,0:T(8,128)(2,1)}, bf16[4,384,128]{2,1,0:T(8,128)(2,1)}, bf16[4,384,128]{2,1,0:T(8,128)(2,1)}, bf16[4,384,128]{2,1,0:T(8,128)(2,1)}) custom-call(s32[1]{0:T(128)} %bitcast.lane, bf16[4,4,256,128]{3,2,1,0:T(8,128)(2,1)} %bitcast.20, bf16[4,4,128,128]{3,2,1,0:T(8,128)(2,1)} %bitcast.21), custom_call_target="tpu_custom_call" | custom-call | tf_op jit(solution)/shard_map/pallas_call | solution.py:50
  130.1 4.2 %collective-permute-start = (bf16[4,384,128]{2,1,0:T(8,128)(2,1)}, bf16[4,384,128]{2,1,0:T(8,128)(2,1)S(1)}, u32[]{:S(2)}, u32[]{:S(2)}) collective-permute-start(bf16[4,384,128]{2,1,0:T(8,128)(2,1)} %get-tuple-element.20), channel_id=1, source_target_pairs={{0,1},{1,2},{2,3},{3,0},{4,5},{5,6},{6,7},{7,4},{8,9},{9,10},{10,1... | collective-permute-start | bytes 1179656 | tf_op jit(solution)/shard_map/ppermute | solution.py:382
  134.3 2.5 %collective-permute-start.1 = (bf16[4,384,128]{2,1,0:T(8,128)(2,1)}, bf16[4,384,128]{2,1,0:T(8,128)(2,1)S(1)}, u32[]{:S(2)}, u32[]{:S(2)}) collective-permute-start(bf16[4,384,128]{2,1,0:T(8,128)(2,1)} %get-tuple-element.21), channel_id=1, source_target_pairs={{0,2},{1,3},{2,0},{3,1},{4,6},{5,7},{6,4},{7,5},{8,10},{9,11},{10,... | collective-permute-start | bytes 1179656 | tf_op jit(solution)/shard_map/ppermute | solution.py:382
  136.8 2.2 %collective-permute-start.2 = (bf16[4,384,128]{2,1,0:T(8,128)(2,1)}, bf16[4,384,128]{2,1,0:T(8,128)(2,1)S(1)}, u32[]{:S(2)}, u32[]{:S(2)}) collective-permute-start(bf16[4,384,128]{2,1,0:T(8,128)(2,1)} %get-tuple-element.22), channel_id=1, source_target_pairs={{0,3},{1,0},{2,1},{3,2},{4,7},{5,4},{6,5},{7,6},{8,11},{9,8},{10,9... | collective-permute-start | bytes 1179656 | tf_op jit(solution)/shard_map/ppermute | solution.py:382
  139.0 5.2 %collective-permute-done.w_1 = bf16[4,384,128]{2,1,0:T(8,128)(2,1)S(1)} collective-permute-done((bf16[4,384,128]{2,1,0:T(8,128)(2,1)}, bf16[4,384,128]{2,1,0:T(8,128)(2,1)S(1)}, u32[]{:S(2)}, u32[]{:S(2)}) %collective-permute-start) | collective-permute-done | bytes 393248 | tf_op jit(solution)/shard_map/ppermute | solution.py:382
  144.2 5.7 %collective-permute-done.1.w_2 = bf16[4,384,128]{2,1,0:T(8,128)(2,1)S(1)} collective-permute-done((bf16[4,384,128]{2,1,0:T(8,128)(2,1)}, bf16[4,384,128]{2,1,0:T(8,128)(2,1)S(1)}, u32[]{:S(2)}, u32[]{:S(2)}) %collective-permute-start.1) | collective-permute-done | bytes 393248 | tf_op jit(solution)/shard_map/ppermute | solution.py:382
  149.9 5.5 %collective-permute-done.2.w_3 = bf16[4,384,128]{2,1,0:T(8,128)(2,1)S(1)} collective-permute-done((bf16[4,384,128]{2,1,0:T(8,128)(2,1)}, bf16[4,384,128]{2,1,0:T(8,128)(2,1)S(1)}, u32[]{:S(2)}, u32[]{:S(2)}) %collective-permute-start.2) | collective-permute-done | bytes 393248 | tf_op jit(solution)/shard_map/ppermute | solution.py:382
  155.4 1.0 copy-done
  156.4 1.0 shard_map.147
  157.4 14.7 %all_to_all.26.parts = bf16[4,768,128]{2,1,0:T(8,128)(2,1)S(1)} all-to-all(bf16[4,768,128]{2,1,0:T(8,128)(2,1)S(1)} %shard_map.147), channel_id=1, replica_groups=mesh['ep_0'=8,'ep_1'=2,'ep_2'=2,'tp_0'=4,'tp_1'=4] {'tp_1'}, dimensions={0} | all-to-all | bytes 1572864 | tf_op jit(solution)/shard_map/all_to_all | solution.py:478
  172.1 0.7 shard_map.148
  172.9 8.1 %all-to-all-start.4 = ((bf16[32,16,128]{2,1,0:T(8,128)(2,1)}), bf16[32,16,128]{2,1,0:T(8,128)(2,1)S(1)}, u32[]{:S(2)}, u32[]{:S(2)}) async-start(bf16[32,16,128]{2,1,0:T(8,128)(2,1)} %get-tuple-element.24), calls=%async_computation.4 | async-start | bytes 262144 | tf_op jit(solution)/shard_map/all_to_all | solution.py:486
  181.3 16.9 %all-to-all-done.4.back = bf16[32,16,128]{2,1,0:T(8,128)(2,1)S(1)} async-done(((bf16[32,16,128]{2,1,0:T(8,128)(2,1)}), bf16[32,16,128]{2,1,0:T(8,128)(2,1)S(1)}, u32[]{:S(2)}, u32[]{:S(2)}) %all-to-all-start.4) | async-done | bytes 131104 | tf_op jit(solution)/shard_map/all_to_all | solution.py:486
  198.2 1.0 shard_map.149
  (22 shorter events, 1.0 us)
Async XLA Ops:
  37.2 8.3 %copy-start.1 = (bf16[256,128]{1,0:T(8,128)(2,1)S(1)}, bf16[256,128]{1,0:T(8,128)(2,1)}, u32[]{:S(2)}) copy-start(bf16[256,128]{1,0:T(8,128)(2,1)} %q.1) | copy-start | bytes 196612
  37.2 8.3 %copy-start.2 = (bf16[256,128]{1,0:T(8,128)(2,1)S(1)}, bf16[256,128]{1,0:T(8,128)(2,1)}, u32[]{:S(2)}) copy-start(bf16[256,128]{1,0:T(8,128)(2,1)} %k.1) | copy-start | bytes 196612
  37.2 8.3 %copy-start.3 = (bf16[256,128]{1,0:T(8,128)(2,1)S(1)}, bf16[256,128]{1,0:T(8,128)(2,1)}, u32[]{:S(2)}) copy-start(bf16[256,128]{1,0:T(8,128)(2,1)} %v.1) | copy-start | bytes 196612
  37.2 8.3 %copy-start.5 = (f32[256,1]{0,1:T(1,128)S(1)}, f32[256,1]{0,1:T(1,128)}, u32[]{:S(2)}) copy-start(f32[256,1]{0,1:T(1,128)} %param.17) | copy-start | bytes 3076
  37.2 33.1 %copy-start.4 = (bf16[256,128]{1,0:T(8,128)(2,1)S(1)}, bf16[256,128]{1,0:T(8,128)(2,1)}, u32[]{:S(2)}) copy-start(bf16[256,128]{1,0:T(8,128)(2,1)} %gates.1) | copy-start | bytes 196612
  37.2 34.5 %all-to-all-start.1 = ((bf16[16,512,128]{2,1,0:T(8,128)(2,1)}), bf16[16,512,128]{2,1,0:T(8,128)(2,1)S(1)}, u32[]{:S(2)}, u32[]{:S(2)}) async-start(bf16[16,512,128]{2,1,0:T(8,128)(2,1)} %shard_map.141), calls=%async_computation.1 | async-start | bytes 4194304 | tf_op jit(solution)/shard_map/all_to_all | solution.py:449
  77.0 78.4 %all-to-all-start.2 = ((bf16[4,1280,128]{2,1,0:T(8,128)(2,1)}), bf16[4,1280,128]{2,1,0:T(8,128)(2,1)S(1)}, u32[]{:S(2)}, u32[]{:S(2)}) async-start(bf16[4,1280,128]{2,1,0:T(8,128)(2,1)} %shard_map.145), calls=%async_computation.2 | async-start | bytes 2621440 | tf_op jit(solution)/shard_map/all_to_all | solution.py:469
  130.1 14.1 %collective-permute-start = (bf16[4,384,128]{2,1,0:T(8,128)(2,1)}, bf16[4,384,128]{2,1,0:T(8,128)(2,1)S(1)}, u32[]{:S(2)}, u32[]{:S(2)}) collective-permute-start(bf16[4,384,128]{2,1,0:T(8,128)(2,1)} %get-tuple-element.20), channel_id=1, source_target_pairs={{0,1},{1,2},{2,3},{3,0},{4,5},{5,6},{6,7},{7,4},{8,9},{9,10},{10,1... | collective-permute-start | bytes 1179656 | tf_op jit(solution)/shard_map/ppermute | solution.py:382
  134.3 15.6 %collective-permute-start.1 = (bf16[4,384,128]{2,1,0:T(8,128)(2,1)}, bf16[4,384,128]{2,1,0:T(8,128)(2,1)S(1)}, u32[]{:S(2)}, u32[]{:S(2)}) collective-permute-start(bf16[4,384,128]{2,1,0:T(8,128)(2,1)} %get-tuple-element.21), channel_id=1, source_target_pairs={{0,2},{1,3},{2,0},{3,1},{4,6},{5,7},{6,4},{7,5},{8,10},{9,11},{10,... | collective-permute-start | bytes 1179656 | tf_op jit(solution)/shard_map/ppermute | solution.py:382
  136.8 18.6 %collective-permute-start.2 = (bf16[4,384,128]{2,1,0:T(8,128)(2,1)}, bf16[4,384,128]{2,1,0:T(8,128)(2,1)S(1)}, u32[]{:S(2)}, u32[]{:S(2)}) collective-permute-start(bf16[4,384,128]{2,1,0:T(8,128)(2,1)} %get-tuple-element.22), channel_id=1, source_target_pairs={{0,3},{1,0},{2,1},{3,2},{4,7},{5,4},{6,5},{7,6},{8,11},{9,8},{10,9... | collective-permute-start | bytes 1179656 | tf_op jit(solution)/shard_map/ppermute | solution.py:382
  155.4 1.0 copy-start
  157.4 23.7 %copy-start.6 = (f32[256,2]{0,1:T(2,128)S(1)}, f32[256,2]{0,1:T(2,128)}, u32[]{:S(2)}) copy-start(f32[256,2]{0,1:T(2,128)} %param.22) | copy-start | bytes 6148
  172.9 25.3 %all-to-all-start.4 = ((bf16[32,16,128]{2,1,0:T(8,128)(2,1)}), bf16[32,16,128]{2,1,0:T(8,128)(2,1)S(1)}, u32[]{:S(2)}, u32[]{:S(2)}) async-start(bf16[32,16,128]{2,1,0:T(8,128)(2,1)} %get-tuple-element.24), calls=%async_computation.4 | async-start | bytes 262144 | tf_op jit(solution)/shard_map/all_to_all | solution.py:486

commit v3 on v2

--- a/solution.py
+++ b/solution.py
@@ -151,50 +151,73 @@
                 pltpu.make_async_copy(w_up.at[0, span], near_up.at[span], sems.at[1, k]),
             )
         )
-    for one, two in copies:
-        one.start()
-        two.start()
+    for kind in range(2):
+        for pair in copies:
+            pair[kind].start()
     near[2 * count :, :] = heads[...]
-    gate = jnp.zeros((count, w_gate.shape[2]), F32)
-    up = gate
     per = parts // chunks
-    for k in range(chunks):
-        left = jnp.concatenate([rows[k * per + j] for j in range(per)], axis=1)
-        span = slice(k * tall, (k + 1) * tall)
-        copies[k][0].wait()
-        gate += dot(left, near_gate[span, :])
-        copies[k][1].wait()
-        up += dot(left, near_up[span, :])
-    hidden = (gate / (1.0 + jnp.exp(-gate)) * up).astype(BF)
-    near[0:count, :] = hidden[:, 0:HEAD]
-    near[count : 2 * count, :] = hidden[:, HEAD:]
-    final = [pltpu.make_async_copy(near, out.at[k], ends.at[k]) for k in range(copied)]
-    for copy in final:
-        copy.start()
+    half = count // 2
+    final = []
+    for side in range(2):
+        span = slice(side * half, (side + 1) * half)
+        sums = []
+        for kind, near_w in ((0, near_gate), (1, near_up)):
+            total = jnp.zeros((half, w_gate.shape[2]), F32)
+            for k in range(chunks):
+                if side == 0:
+                    copies[k][kind].wait()
+                left = jnp.concatenate([rows[k * per + j, span, :] for j in range(per)], axis=1)
+                total += dot(left, near_w[k * tall : (k + 1) * tall, :])
+            sums.append(total)
+        gate, up = sums
+        hidden = (gate / (1.0 + jnp.exp(-gate)) * up).astype(BF)
+        for part in range(2):
+            at = part * count + side * half
+            near[at : at + half, :] = hidden[:, part * HEAD : (part + 1) * HEAD]
+            for k in range(copied):
+                here = pl.ds(at, half)
+                copy = pltpu.make_async_copy(
+                    near.at[here], out.at[k, here], ends.at[k, 2 * side + part]
+                )
+                copy.start()
+                final.append(copy)
+        if side == 0:
+            here = pl.ds(2 * count, heads.shape[0])
+            for k in range(copied):
+                copy = pltpu.make_async_copy(near.at[here], out.at[k, here], ends.at[k, 4])
+                copy.start()
+                final.append(copy)
     for copy in final:
         copy.wait()
 
 
-def project_body(lane, got, w_0, w_1, w_2, w_3, out):
+def project_body(lane, got, down, weight, w_1, w_2, w_3, out, own, sems):
     peers = got.shape[0]
     positions = got.shape[1] // 5
     count = 2 * positions
     units = 2 * HEAD
-    near = (w_0, w_1, w_2, w_3)
+    copies = [
+        pltpu.make_async_copy(down.at[:, lane[0]], own.at[:, 0:units], sems.at[0]),
+        pltpu.make_async_copy(weight.at[:, lane[0]], own.at[:, units:], sems.at[1]),
+    ]
+    for copy in copies:
+        copy.start()
     left = [
         jnp.concatenate([got[k, 0:count, :], got[k, count : 2 * count, :]], axis=1)
         for k in range(peers)
     ]
-    for first in (0, 2):
-        one, two = near[first], near[first + 1]
+    for (one, two), steps in (((w_2, w_3), (2, 3)), ((own, w_1), (0, 1))):
+        if steps[0] == 0:
+            for copy in copies:
+                copy.wait()
         expert = jnp.zeros((count, 2 * HEAD), F32)
         mixer = jnp.zeros((positions, 2 * HEAD), F32)
         for k in range(peers):
             both = jnp.concatenate([one[k], two[k]], axis=1)
             expert += dot(left[k], both[0:units])
             mixer += dot(got[k, 2 * count :, :], both[units:])
-        for which in range(2):
-            at = (lane[0] + peers - first - which) % peers
+        for which, step in enumerate(steps):
+            at = (lane[0] + peers - step) % peers
             cols = slice(which * HEAD, which * HEAD + HEAD)
             out[pl.ds(at, 1), 0:count, :] = expert[:, cols].astype(BF)[None]
             out[pl.ds(at, 1), count:, :] = mixer[:, cols].astype(BF)[None]
@@ -330,7 +353,7 @@
         log_decay.reshape(count // BLOCK, BLOCK),
         cosine,
         sine,
-        kinds="hhhhvv",
+        kinds="ppppvv",
         outs="hhv",
     )
     place = lax.axis_index(("ep_1", "ep_2")).reshape(1)
@@ -401,12 +424,13 @@
             scratch=[pltpu.SemaphoreType.DMA((2 * len(steps),))],
         )
 
-    place = pltpu.HBM(shape, BF)
-    one, three, own, two = cut((1, 3, 0, 2), [place] * peers, "aaaa")
-    swapped = [own]
+    place = onchip(shape, BF)
+    one, three = cut((1, 3), [place] * 2, "vv")
+    (two,) = cut((2,), [place], "v")
+    swapped = []
     for far, block in ((1, one), (2, two), (3, three)):
         swapped.append(shifted(block, "tp_1", far))
-    return swapped
+    return [down, heads, *swapped]
 
 
 def both_halves(
@@ -463,7 +487,7 @@
             pltpu.VMEM((width, units), BF),
             pltpu.VMEM((tall, HEAD), BF),
             pltpu.SemaphoreType.DMA((2, 8)),
-            pltpu.SemaphoreType.DMA((rows_y,)),
+            pltpu.SemaphoreType.DMA((rows_y, 5)),
         ],
     )
     got = lax.all_to_all(mixed, "tp_0", 0, 0, tiled=True)
@@ -473,7 +497,8 @@
         lane.reshape(1),
         got,
         *weights,
-        kinds="svhhhh",
+        kinds="svaahhh",
+        scratch=[pltpu.VMEM(weights[-1].shape, BF), pltpu.SemaphoreType.DMA((2,))],
     )
     pieces = lax.all_to_all(partial, "tp_1", 0, 0, tiled=True)
     summed, mixer_out = call(

time: 201 us -> 154 us (0.77)
  Pallas kernels: 63.9 us -> 18.1 us
    pallas_call x10 -> x11, Pallas kernels: 63.9 us -> 18.1 us  [call(): pl.pallas_call(body, in_specs=[places[kind] for kind in kinds], out_specs...]
  transfers between devices with their start and end apart: 6 -> 6, of which waited for: 4 -> 4; matrix products, arithmetic and copies ran while one was open for 0% -> 1% of each run, Pallas kernels for 26% -> 4%
where the time goes in v3:
time: 154 us; the launch traced here: 151 us
  blocking collectives  70.4 us (46%)
  waiting for transfers between devices  33.4 us (22%)
  starting transfers between devices  27.7 us (18%)
  Pallas kernels  18.1 us (12%)
    all_to_all x1, blocking collectives, both_halves(): arrived = lax.all_to_all(send, EP, 0, 0, tiled=True)  32.5 us
    pallas_call x11, Pallas kernels, call(): pl.pallas_call(body, in_specs=[places[kind] for kind in kinds], out_specs...  18.1 us
    all_gather x1, blocking collectives, retention_heads(): far = lax.all_gather(pay, ('ep_0', 'ep_2'))  17.8 us
    all_to_all x1, waiting for transfers between devices, both_halves(): back = lax.all_to_all(summed, EP, 0, 0, tiled=True)  16.9 us
    ppermute x3, waiting for transfers between devices, shifted(): lax.ppermute(array, axis, [(k, (k + far) % peers) for k in range(peers)])  16.5 us
    all_to_all x1, blocking collectives, both_halves(): pieces = lax.all_to_all(partial, 'tp_1', 0, 0, tiled=True)  14.7 us
    ppermute x3, starting transfers between devices, shifted(): lax.ppermute(array, axis, [(k, (k + far) % peers) for k in range(peers)])  8.63 us
    all_to_all x1, starting transfers between devices, both_halves(): rows = lax.all_to_all(spread, TP, 0, 0, tiled=True)  7.57 us
  transfers between devices with their start and end apart: 6, of which 4 were waited for; matrix products, arithmetic and copies ran while one was open for 1% of the time, Pallas kernels for 4%

profile of v3, /device:TPU:6, one launch (start us, length us, event | category | flops | bytes accessed | tf_op | source)
XLA Modules:
  0.0 151.2 jit_solution(18393643877483774165)
XLA Ops:
  0.6 2.6 %shard_map.140 = (bf16[32,16,128]{2,1,0:T(8,128)(2,1)S(1)}, s32[2,256]{1,0:T(2,128)S(1)}) custom-call(s32[1]{0:T(128)} %bitcast.1.turn, s32[2,256]{1,0:T(2,128)} %bitcast.26, bf16[16,128]{1,0:T(8,128)(2,1)} %bitcast.25, bf16[256,2048]{1,0:T(8,128)(2,1)} %source.1), custom_call_target="tpu_custom_call" | custom-call | tf_op jit(solution)/shard_map/pallas_call | solution.py:50
  3.2 32.5 %all_to_all.25 = bf16[32,16,128]{2,1,0:T(8,128)(2,1)S(1)} all-to-all(bf16[32,16,128]{2,1,0:T(8,128)(2,1)S(1)} %get-tuple-element.13), channel_id=1, replica_groups=mesh['ep_0'=8,'ep_1'=2,'ep_2'=2,'tp_0'=4,'tp_1'=4] {'ep_0','ep_1','ep_2'}, dimensions={0} | all-to-all | bytes 262144 | tf_op jit(solution)/shard_map/all_to_all | solution.py:464
  35.7 1.5 shard_map.141
  37.2 7.6 %all-to-all-start.1 = ((bf16[16,512,128]{2,1,0:T(8,128)(2,1)}), bf16[16,512,128]{2,1,0:T(8,128)(2,1)S(1)}, u32[]{:S(2)}, u32[]{:S(2)}) async-start(bf16[16,512,128]{2,1,0:T(8,128)(2,1)} %shard_map.141), calls=%async_computation.1 | async-start | bytes 4194304 | tf_op jit(solution)/shard_map/all_to_all | solution.py:473
  45.4 2.5 %shard_map.142 = (f32[256,128]{1,0:T(8,128)}, f32[256,128]{1,0:T(8,128)}, bf16[144,128]{1,0:T(8,128)(2,1)S(1)}) custom-call(bf16[256,128]{1,0:T(8,128)(2,1)} %q.1, bf16[256,128]{1,0:T(8,128)(2,1)} %k.1, bf16[256,128]{1,0:T(8,128)(2,1)} %v.1, f32[2,128]{1,0:T(2,128)} %bitcast.27, f32[256,128]{1,0:T(8,128)S(1)} %get-tuple-element.25.cosine, ...), custom_call_target="tpu_custom_call" | custom-call | tf_op jit(solution)/shard_map/pallas_call | solution.py:50
  47.9 5.4 %all-gather = bf16[576,128]{1,0:T(8,128)(2,1)S(1)} all-gather(bf16[144,128]{1,0:T(8,128)(2,1)S(1)} %get-tuple-element.14), channel_id=2, replica_groups=mesh['ep_0'=8,'ep_1'=2,'ep_2'=2,'tp_0'=4,'tp_1'=4] {'ep_1','ep_2'}, dimensions={0}, use_global_device_ids=true | all-gather | bytes 184320 | tf_op jit(solution)/shard_map/all_gather | solution.py:360
  53.4 17.8 %all-gather.1 = bf16[1280,128]{1,0:T(8,128)(2,1)S(1)} all-gather(bf16[80,128]{1,0:T(8,128)(2,1)S(1)} %shard_map.143), channel_id=3, replica_groups=mesh['ep_0'=8,'ep_1'=2,'ep_2'=2,'tp_0'=4,'tp_1'=4] {'ep_0','ep_2'}, dimensions={0}, use_global_device_ids=true | all-gather | bytes 348160 | tf_op jit(solution)/shard_map/all_gather | solution.py:368
  71.2 1.4 shard_map.144.heads
  72.6 4.5 %shard_map.145 = bf16[4,1280,128]{2,1,0:T(8,128)(2,1)} custom-call(bf16[16,512,128]{2,1,0:T(8,128)(2,1)S(1)} %all-to-all-done.1.rows, bf16[256,128]{1,0:T(8,128)(2,1)S(1)} %shard_map.144.heads, bf16[1,2048,256]{2,1,0:T(8,128)(2,1)} %w_gate.1, bf16[1,2048,256]{2,1,0:T(8,128)(2,1)} %w_up.1), custom_call_target="tpu_custom_call" | custom-call | tf_op jit(solution)/shard_map/pallas_call | solution.py:50
  77.1 4.3 %all-to-all-start.2 = ((bf16[4,1280,128]{2,1,0:T(8,128)(2,1)}), bf16[4,1280,128]{2,1,0:T(8,128)(2,1)S(1)}, u32[]{:S(2)}, u32[]{:S(2)}) async-start(bf16[4,1280,128]{2,1,0:T(8,128)(2,1)} %shard_map.145), calls=%async_computation.2 | async-start | bytes 2621440 | tf_op jit(solution)/shard_map/all_to_all | solution.py:493
  81.4 1.2 shard_map.146
  82.5 3.3 %collective-permute-start = (bf16[4,384,128]{2,1,0:T(8,128)(2,1)S(1)}, bf16[4,384,128]{2,1,0:T(8,128)(2,1)S(1)}, u32[]{:S(2)}, u32[]{:S(2)}) collective-permute-start(bf16[4,384,128]{2,1,0:T(8,128)(2,1)S(1)} %get-tuple-element.17), channel_id=1, source_target_pairs={{0,1},{1,2},{2,3},{3,0},{4,5},{5,6},{6,7},{7,4},{8,9},{9,10},{10,1... | collective-permute-start | bytes 1179656 | tf_op jit(solution)/shard_map/ppermute | solution.py:405
  85.9 1.0 shard_map.147
  86.9 3.4 %collective-permute-start.1 = (bf16[4,384,128]{2,1,0:T(8,128)(2,1)S(1)}, bf16[4,384,128]{2,1,0:T(8,128)(2,1)S(1)}, u32[]{:S(2)}, u32[]{:S(2)}) collective-permute-start(bf16[4,384,128]{2,1,0:T(8,128)(2,1)S(1)} %shard_map.147), channel_id=1, source_target_pairs={{0,2},{1,3},{2,0},{3,1},{4,6},{5,7},{6,4},{7,5},{8,10},{9,11},{10,... | collective-permute-start | bytes 1179656 | tf_op jit(solution)/shard_map/ppermute | solution.py:405
  90.3 1.9 %collective-permute-start.2 = (bf16[4,384,128]{2,1,0:T(8,128)(2,1)S(1)}, bf16[4,384,128]{2,1,0:T(8,128)(2,1)S(1)}, u32[]{:S(2)}, u32[]{:S(2)}) collective-permute-start(bf16[4,384,128]{2,1,0:T(8,128)(2,1)S(1)} %get-tuple-element.18), channel_id=1, source_target_pairs={{0,3},{1,0},{2,1},{3,2},{4,7},{5,4},{6,5},{7,6},{8,11},{9,8},{10,9... | collective-permute-start | bytes 1179656 | tf_op jit(solution)/shard_map/ppermute | solution.py:405
  92.2 4.2 %collective-permute-done.w_1 = bf16[4,384,128]{2,1,0:T(8,128)(2,1)S(1)} collective-permute-done((bf16[4,384,128]{2,1,0:T(8,128)(2,1)S(1)}, bf16[4,384,128]{2,1,0:T(8,128)(2,1)S(1)}, u32[]{:S(2)}, u32[]{:S(2)}) %collective-permute-start) | collective-permute-done | bytes 393248 | tf_op jit(solution)/shard_map/ppermute | solution.py:405
  96.4 5.9 %collective-permute-done.1.w_2 = bf16[4,384,128]{2,1,0:T(8,128)(2,1)S(1)} collective-permute-done((bf16[4,384,128]{2,1,0:T(8,128)(2,1)S(1)}, bf16[4,384,128]{2,1,0:T(8,128)(2,1)S(1)}, u32[]{:S(2)}, u32[]{:S(2)}) %collective-permute-start.1) | collective-permute-done | bytes 393248 | tf_op jit(solution)/shard_map/ppermute | solution.py:405
  102.3 6.4 %collective-permute-done.2.w_3 = bf16[4,384,128]{2,1,0:T(8,128)(2,1)S(1)} collective-permute-done((bf16[4,384,128]{2,1,0:T(8,128)(2,1)S(1)}, bf16[4,384,128]{2,1,0:T(8,128)(2,1)S(1)}, u32[]{:S(2)}, u32[]{:S(2)}) %collective-permute-start.2) | collective-permute-done | bytes 393248 | tf_op jit(solution)/shard_map/ppermute | solution.py:405
  108.7 1.7 %shard_map.148 = bf16[4,768,128]{2,1,0:T(8,128)(2,1)S(1)} custom-call(s32[1]{0:T(128)} %bitcast.lane, bf16[4,1280,128]{2,1,0:T(8,128)(2,1)S(1)} %all-to-all-done.2.got, bf16[4,4,256,128]{3,2,1,0:T(8,128)(2,1)} %bitcast.21, bf16[4,4,128,128]{3,2,1,0:T(8,128)(2,1)} %bitcast.24, bf16[4,384,128]{2,1,0:T(8,128)(2,1)S(1)} %collective-permute-done.w_1, ...), custom_call_target="tpu_custom_call" | custom-call | tf_op jit(solution)/shard_map/pallas_call | solution.py:50
  110.4 14.7 %all_to_all.26.parts = bf16[4,768,128]{2,1,0:T(8,128)(2,1)S(1)} all-to-all(bf16[4,768,128]{2,1,0:T(8,128)(2,1)S(1)} %shard_map.148), channel_id=1, replica_groups=mesh['ep_0'=8,'ep_1'=2,'ep_2'=2,'tp_0'=4,'tp_1'=4] {'tp_1'}, dimensions={0} | all-to-all | bytes 1572864 | tf_op jit(solution)/shard_map/all_to_all | solution.py:503
  125.1 0.7 shard_map.149
  125.8 7.2 %all-to-all-start.4 = ((bf16[32,16,128]{2,1,0:T(8,128)(2,1)}), bf16[32,16,128]{2,1,0:T(8,128)(2,1)S(1)}, u32[]{:S(2)}, u32[]{:S(2)}) async-start(bf16[32,16,128]{2,1,0:T(8,128)(2,1)} %get-tuple-element.20), calls=%async_computation.4 | async-start | bytes 262144 | tf_op jit(solution)/shard_map/all_to_all | solution.py:511
  133.4 16.9 %all-to-all-done.4.back = bf16[32,16,128]{2,1,0:T(8,128)(2,1)S(1)} async-done(((bf16[32,16,128]{2,1,0:T(8,128)(2,1)}), bf16[32,16,128]{2,1,0:T(8,128)(2,1)S(1)}, u32[]{:S(2)}, u32[]{:S(2)}) %all-to-all-start.4) | async-done | bytes 131104 | tf_op jit(solution)/shard_map/all_to_all | solution.py:511
  150.3 1.0 shard_map.150
  (13 shorter events, 1.0 us)
Async XLA Ops:
  37.2 34.0 %copy-start = (bf16[256,128]{1,0:T(8,128)(2,1)S(1)}, bf16[256,128]{1,0:T(8,128)(2,1)}, u32[]{:S(2)}) copy-start(bf16[256,128]{1,0:T(8,128)(2,1)} %gates.1) | copy-start | bytes 196612
  37.2 35.4 %all-to-all-start.1 = ((bf16[16,512,128]{2,1,0:T(8,128)(2,1)}), bf16[16,512,128]{2,1,0:T(8,128)(2,1)S(1)}, u32[]{:S(2)}, u32[]{:S(2)}) async-start(bf16[16,512,128]{2,1,0:T(8,128)(2,1)} %shard_map.141), calls=%async_computation.1 | async-start | bytes 4194304 | tf_op jit(solution)/shard_map/all_to_all | solution.py:473
  77.1 31.6 %all-to-all-start.2 = ((bf16[4,1280,128]{2,1,0:T(8,128)(2,1)}), bf16[4,1280,128]{2,1,0:T(8,128)(2,1)S(1)}, u32[]{:S(2)}, u32[]{:S(2)}) async-start(bf16[4,1280,128]{2,1,0:T(8,128)(2,1)} %shard_map.145), calls=%async_computation.2 | async-start | bytes 2621440 | tf_op jit(solution)/shard_map/all_to_all | solution.py:493
  82.5 13.9 %collective-permute-start = (bf16[4,384,128]{2,1,0:T(8,128)(2,1)S(1)}, bf16[4,384,128]{2,1,0:T(8,128)(2,1)S(1)}, u32[]{:S(2)}, u32[]{:S(2)}) collective-permute-start(bf16[4,384,128]{2,1,0:T(8,128)(2,1)S(1)} %get-tuple-element.17), channel_id=1, source_target_pairs={{0,1},{1,2},{2,3},{3,0},{4,5},{5,6},{6,7},{7,4},{8,9},{9,10},{10,1... | collective-permute-start | bytes 1179656 | tf_op jit(solution)/shard_map/ppermute | solution.py:405
  86.9 15.4 %collective-permute-start.1 = (bf16[4,384,128]{2,1,0:T(8,128)(2,1)S(1)}, bf16[4,384,128]{2,1,0:T(8,128)(2,1)S(1)}, u32[]{:S(2)}, u32[]{:S(2)}) collective-permute-start(bf16[4,384,128]{2,1,0:T(8,128)(2,1)S(1)} %shard_map.147), channel_id=1, source_target_pairs={{0,2},{1,3},{2,0},{3,1},{4,6},{5,7},{6,4},{7,5},{8,10},{9,11},{10,... | collective-permute-start | bytes 1179656 | tf_op jit(solution)/shard_map/ppermute | solution.py:405
  90.3 18.4 %collective-permute-start.2 = (bf16[4,384,128]{2,1,0:T(8,128)(2,1)S(1)}, bf16[4,384,128]{2,1,0:T(8,128)(2,1)S(1)}, u32[]{:S(2)}, u32[]{:S(2)}) collective-permute-start(bf16[4,384,128]{2,1,0:T(8,128)(2,1)S(1)} %get-tuple-element.18), channel_id=1, source_target_pairs={{0,3},{1,0},{2,1},{3,2},{4,7},{5,4},{6,5},{7,6},{8,11},{9,8},{10,9... | collective-permute-start | bytes 1179656 | tf_op jit(solution)/shard_map/ppermute | solution.py:405
  110.4 22.8 %copy-start.1 = (f32[256,2]{0,1:T(2,128)S(1)}, f32[256,2]{0,1:T(2,128)}, u32[]{:S(2)}) copy-start(f32[256,2]{0,1:T(2,128)} %param.22) | copy-start | bytes 6148
  125.8 24.4 %all-to-all-start.4 = ((bf16[32,16,128]{2,1,0:T(8,128)(2,1)}), bf16[32,16,128]{2,1,0:T(8,128)(2,1)S(1)}, u32[]{:S(2)}, u32[]{:S(2)}) async-start(bf16[32,16,128]{2,1,0:T(8,128)(2,1)} %get-tuple-element.20), calls=%async_computation.4 | async-start | bytes 262144 | tf_op jit(solution)/shard_map/all_to_all | solution.py:511

commit v4 on v3

--- a/solution.py
+++ b/solution.py
@@ -191,7 +191,7 @@
         copy.wait()
 
 
-def project_body(lane, got, down, weight, w_1, w_2, w_3, out, own, sems):
+def project_body(lane, got, down, weight, w_1, w_2, w_3, out, m_0, m_1, m_2, m_3, own, sems):
     peers = got.shape[0]
     positions = got.shape[1] // 5
     count = 2 * positions
@@ -206,6 +206,7 @@
         jnp.concatenate([got[k, 0:count, :], got[k, count : 2 * count, :]], axis=1)
         for k in range(peers)
     ]
+    mixes = (m_0, m_1, m_2, m_3)
     for (one, two), steps in (((w_2, w_3), (2, 3)), ((own, w_1), (0, 1))):
         if steps[0] == 0:
             for copy in copies:
@@ -219,17 +220,22 @@
         for which, step in enumerate(steps):
             at = (lane[0] + peers - step) % peers
             cols = slice(which * HEAD, which * HEAD + HEAD)
-            out[pl.ds(at, 1), 0:count, :] = expert[:, cols].astype(BF)[None]
-            out[pl.ds(at, 1), count:, :] = mixer[:, cols].astype(BF)[None]
-
-
-def add_body(parts, experts, mixer):
+            out[pl.ds(at, 1)] = expert[:, cols].astype(BF)[None]
+            mixes[step][...] = mixer[:, cols].astype(BF)
+
+
+def add_body(parts, out):
     total = parts[0].astype(F32)
     for k in range(1, parts.shape[0]):
         total += parts[k].astype(F32)
-    count = experts.shape[0] * experts.shape[1]
-    experts[...] = total[0:count].astype(BF).reshape(experts.shape)
-    mixer[...] = total[count:].astype(BF)
+    out[...] = total.astype(BF).reshape(out.shape)
+
+
+def add_four_body(p_0, p_1, p_2, p_3, out):
+    out[...] = (
+        (p_0[...].astype(F32) + p_1[...].astype(F32))
+        + (p_2[...].astype(F32) + p_3[...].astype(F32))
+    ).astype(BF)
 
 
 def combine_body(back, slots, weights, out):
@@ -319,7 +325,24 @@
     packed(pay, mine, decay)
 
 
-def head_body(place, group, far, near, base, q_decayed, gates, out):
+def head_body(
+    place, group, lane, far, near, base, q_decayed, gates, down, weight, out, b_1, b_3, here, sems
+):
+    peers = down.shape[1]
+    units = down.shape[2]
+    loads, stores = [], []
+    for k, (step, block) in enumerate(((1, b_1), (3, b_3))):
+        at = (lane[0] + step) % peers
+        loads.append(
+            (
+                pltpu.make_async_copy(down.at[:, at], here.at[k, :, 0:units], sems.at[3 * k]),
+                pltpu.make_async_copy(weight.at[:, at], here.at[k, :, units:], sems.at[3 * k + 1]),
+            )
+        )
+        stores.append(pltpu.make_async_copy(here.at[k], block, sems.at[3 * k + 2]))
+    for one, two in loads:
+        one.start()
+        two.start()
     entering = jnp.zeros((HEAD, HEAD), F32)
     for k in range(far.shape[0] // 2):
         upper, decay = unpacked(far.at[2 * k])
@@ -329,13 +352,19 @@
     for k in range(near.shape[0] - 1):
         state, decay = unpacked(near.at[k])
         entering = jnp.where(k < place[0], jnp.exp(decay) * entering + state, entering)
+    for (one, two), store in zip(loads, stores, strict=True):
+        one.wait()
+        two.wait()
+        store.start()
     retained = base[...] + dot(q_decayed[...], entering, precision=HIGH)
     power = jnp.mean(retained * retained, axis=-1, keepdims=True)
     gate = gates[...].astype(F32)
     out[...] = (retained * lax.rsqrt(power + 1e-05) * (gate / (1.0 + jnp.exp(-gate)))).astype(BF)
-
-
-def retention_heads(queries, keys, values, gates, log_decay):
+    for store in stores:
+        store.wait()
+
+
+def retention_heads(queries, keys, values, gates, log_decay, lane, down, weight):
     count = queries.shape[0]
     positions = (lax.axis_index(EP) * count + jnp.arange(count, dtype=jnp.int32)).astype(F32)
     half = HEAD // 2
@@ -365,19 +394,24 @@
         near,
         kinds="sv",
     )
+    block = (down.shape[0], down.shape[2] + weight.shape[2], HEAD)
     far = lax.all_gather(pay, ("ep_0", "ep_2"))
     return call(
         head_body,
-        shaped((count, HEAD), BF),
+        [shaped((count, HEAD), BF), pltpu.HBM(block, BF), pltpu.HBM(block, BF)],
         place,
         lax.axis_index("ep_0").reshape(1),
+        lane.reshape(1),
         far,
         near,
         base,
         q_decayed,
         gates,
-        kinds="sshhpph",
-        outs="h",
+        down,
+        weight,
+        kinds="ssshhpphaa",
+        outs="haa",
+        scratch=[pltpu.VMEM((2, *block), BF), pltpu.SemaphoreType.DMA((6,))],
     )
 
 
@@ -405,32 +439,25 @@
     return lax.ppermute(array, axis, [(k, (k + far) % peers) for k in range(peers)])
 
 
-def exchanged_weights(down_proj, out_weight, lane):
-    peers = lax.axis_size("tp_1")
-    rows = lax.axis_size("tp_0")
-    down = down_proj.reshape(rows, peers, -1, HEAD)
-    heads = out_weight.reshape(rows, peers, -1, HEAD)
-    shape = (rows, down.shape[2] + heads.shape[2], HEAD)
-
-    def cut(steps, outs, places):
-        return call(
-            functools.partial(cut_body, steps),
-            outs,
-            lane.reshape(1),
-            down,
-            heads,
-            kinds="saa",
-            outs=places,
-            scratch=[pltpu.SemaphoreType.DMA((2 * len(steps),))],
-        )
-
-    place = onchip(shape, BF)
-    one, three = cut((1, 3), [place] * 2, "vv")
-    (two,) = cut((2,), [place], "v")
+def by_peer(array, rows, peers):
+    return array.reshape(rows, peers, -1, HEAD)
+
+
+def exchanged_weights(down, weight, one, three, lane):
+    shape = one.shape
+    two = call(
+        functools.partial(cut_body, (2,)),
+        onchip(shape, BF),
+        lane.reshape(1),
+        down,
+        weight,
+        kinds="saa",
+        scratch=[pltpu.SemaphoreType.DMA((2,))],
+    )
     swapped = []
     for far, block in ((1, one), (2, two), (3, three)):
         swapped.append(shifted(block, "tp_1", far))
-    return [down, heads, *swapped]
+    return [down, weight, *swapped]
 
 
 def both_halves(
@@ -460,7 +487,8 @@
     units = gate_proj.shape[2]
     tall = 2 * count + positions
     send, slots = dispatch(moe_rows, moe_gain, routes, experts, lax.axis_index(TP).reshape(1))
-    weights = exchanged_weights(down_proj, out_weight, lane)
+    down = by_peer(down_proj, rows_y, peers)
+    weight = by_peer(out_weight, rows_y, peers)
     arrived = lax.all_to_all(send, EP, 0, 0, tiled=True)
     spread = call(
         spread_body,
@@ -471,7 +499,10 @@
         scratch=[pltpu.SemaphoreType.DMA((members,))],
     )
     rows = lax.all_to_all(spread, TP, 0, 0, tiled=True)
-    head_out = retention_heads(queries, keys, values, gates, log_decay)
+    head_out, one, three = retention_heads(
+        queries, keys, values, gates, log_decay, lane, down, weight
+    )
+    weights = exchanged_weights(down, weight, one, three, lane)
     width = gate_proj.shape[1]
     mixed = call(
         hidden_body,
@@ -486,29 +517,30 @@
             pltpu.VMEM((width, units), BF),
             pltpu.VMEM((width, units), BF),
             pltpu.VMEM((tall, HEAD), BF),
-            pltpu.SemaphoreType.DMA((2, 8)),
+            pltpu.SemaphoreType.DMA((2, 2)),
             pltpu.SemaphoreType.DMA((rows_y, 5)),
         ],
     )
     got = lax.all_to_all(mixed, "tp_0", 0, 0, tiled=True)
-    partial = call(
+    partial, *mixes = call(
         project_body,
-        onchip((peers, count + positions, HEAD), BF),
+        [onchip((peers, count, HEAD), BF)] + [shaped((positions, HEAD), BF)] * peers,
         lane.reshape(1),
         got,
         *weights,
         kinds="svaahhh",
+        outs="vhhhh",
         scratch=[pltpu.VMEM(weights[-1].shape, BF), pltpu.SemaphoreType.DMA((2,))],
     )
     pieces = lax.all_to_all(partial, "tp_1", 0, 0, tiled=True)
-    summed, mixer_out = call(
-        add_body,
-        [onchip((experts, room, HEAD), BF), shaped((positions, HEAD), BF)],
-        pieces,
-        kinds="v",
-        outs="vh",
-    )
+    summed = call(add_body, onchip((experts, room, HEAD), BF), pieces, kinds="v")
     back = lax.all_to_all(summed, EP, 0, 0, tiled=True)
+    gathered = [mixes[0]]
+    for far in range(1, peers):
+        gathered.append(shifted(mixes[far], "tp_1", peers - far))
+    mixer_out = call(
+        add_four_body, shaped((positions, HEAD), BF), *gathered, kinds="hhhh", outs="h"
+    )
     columns, scales = lax.optimization_barrier((slots.T, route_weights))
     moe_out = call(
         combine_body, shaped((tokens, HEAD), BF), back, columns, scales, kinds="vvv", outs="h"

time: 154 us -> 150 us (0.974)
  waiting for transfers between devices: 33.4 us -> 22.2 us
  starting transfers between devices: 27.7 us -> 37.1 us
  blocking collectives: 70.4 us -> 67.6 us
    all_to_all x1, waiting for transfers between devices: 16.9 us -> 3 us  [both_halves(): back = lax.all_to_all(summed, EP, 0, 0, tiled=True)]
    ppermute x3 -> x6, starting transfers between devices: 8.63 us -> 19 us  [shifted(): lax.ppermute(array, axis, [(k, (k + far) % peers) for k in range(peers)])]
    all_to_all x1, blocking collectives: 14.7 us -> 11.9 us  [both_halves(): pieces = lax.all_to_all(partial, 'tp_1', 0, 0, tiled=True)]
    ppermute x3 -> x6, waiting for transfers between devices: 16.5 us -> 19.2 us  [shifted(): lax.ppermute(array, axis, [(k, (k + far) % peers) for k in range(peers)])]
  transfers between devices with their start and end apart: 6 -> 9, of which waited for: 4 -> 5; matrix products, arithmetic and copies ran while one was open for 1% -> 1% of each run, Pallas kernels for 4% -> 5%
where the time goes in v4:
time: 150 us; the launch traced here: 148 us
  blocking collectives  67.6 us (45%)
  starting transfers between devices  37.1 us (25%)
  waiting for transfers between devices  22.2 us (15%)
  Pallas kernels  19.3 us (13%)
    all_to_all x1, blocking collectives, both_halves(): arrived = lax.all_to_all(send, EP, 0, 0, tiled=True)  32.5 us
    pallas_call x11, Pallas kernels, call(): pl.pallas_call(body, in_specs=[places[kind] for kind in kinds], out_specs...  19.3 us
    ppermute x6, waiting for transfers between devices, shifted(): lax.ppermute(array, axis, [(k, (k + far) % peers) for k in range(peers)])  19.2 us
    ppermute x6, starting transfers between devices, shifted(): lax.ppermute(array, axis, [(k, (k + far) % peers) for k in range(peers)])  19 us
    all_gather x1, blocking collectives, retention_heads(): far = lax.all_gather(pay, ('ep_0', 'ep_2'))  17.8 us
    all_to_all x1, blocking collectives, both_halves(): pieces = lax.all_to_all(partial, 'tp_1', 0, 0, tiled=True)  11.9 us
    all_to_all x1, starting transfers between devices, both_halves(): rows = lax.all_to_all(spread, TP, 0, 0, tiled=True)  7.57 us
    all_to_all x1, starting transfers between devices, both_halves(): back = lax.all_to_all(summed, EP, 0, 0, tiled=True)  6.09 us
  transfers between devices with their start and end apart: 9, of which 5 were waited for; matrix products, arithmetic and copies ran while one was open for 1% of the time, Pallas kernels for 5%

profile of v4, /device:TPU:6, one launch (start us, length us, event | category | flops | bytes accessed | tf_op | source)
XLA Modules:
  0.0 147.9 jit_solution(4356613464031737693)
XLA Ops:
  0.6 2.6 %shard_map.140 = (bf16[32,16,128]{2,1,0:T(8,128)(2,1)S(1)}, s32[2,256]{1,0:T(2,128)S(1)}) custom-call(s32[1]{0:T(128)} %bitcast.1.turn, s32[2,256]{1,0:T(2,128)} %bitcast.26, bf16[16,128]{1,0:T(8,128)(2,1)} %bitcast.25, bf16[256,2048]{1,0:T(8,128)(2,1)} %source.1), custom_call_target="tpu_custom_call" | custom-call | tf_op jit(solution)/shard_map/pallas_call | solution.py:50
  3.2 32.5 %all_to_all.25 = bf16[32,16,128]{2,1,0:T(8,128)(2,1)S(1)} all-to-all(bf16[32,16,128]{2,1,0:T(8,128)(2,1)S(1)} %get-tuple-element.17), channel_id=1, replica_groups=mesh['ep_0'=8,'ep_1'=2,'ep_2'=2,'tp_0'=4,'tp_1'=4] {'ep_0','ep_1','ep_2'}, dimensions={0} | all-to-all | bytes 262144 | tf_op jit(solution)/shard_map/all_to_all | solution.py:492
  35.7 1.5 shard_map.141
  37.2 7.6 %all-to-all-start.1 = ((bf16[16,512,128]{2,1,0:T(8,128)(2,1)}), bf16[16,512,128]{2,1,0:T(8,128)(2,1)S(1)}, u32[]{:S(2)}, u32[]{:S(2)}) async-start(bf16[16,512,128]{2,1,0:T(8,128)(2,1)} %shard_map.141), calls=%async_computation.1 | async-start | bytes 4194304 | tf_op jit(solution)/shard_map/all_to_all | solution.py:501
  45.4 2.5 %shard_map.142 = (f32[256,128]{1,0:T(8,128)}, f32[256,128]{1,0:T(8,128)}, bf16[144,128]{1,0:T(8,128)(2,1)S(1)}) custom-call(bf16[256,128]{1,0:T(8,128)(2,1)} %q.1, bf16[256,128]{1,0:T(8,128)(2,1)} %k.1, bf16[256,128]{1,0:T(8,128)(2,1)} %v.1, f32[2,128]{1,0:T(2,128)} %bitcast.27, f32[256,128]{1,0:T(8,128)S(1)} %get-tuple-element.33.cosine, ...), custom_call_target="tpu_custom_call" | custom-call | tf_op jit(solution)/shard_map/pallas_call | solution.py:50
  47.9 5.4 %all-gather = bf16[576,128]{1,0:T(8,128)(2,1)S(1)} all-gather(bf16[144,128]{1,0:T(8,128)(2,1)S(1)} %get-tuple-element.18), channel_id=2, replica_groups=mesh['ep_0'=8,'ep_1'=2,'ep_2'=2,'tp_0'=4,'tp_1'=4] {'ep_1','ep_2'}, dimensions={0}, use_global_device_ids=true | all-gather | bytes 184320 | tf_op jit(solution)/shard_map/all_gather | solution.py:389
  53.4 17.8 %all-gather.1 = bf16[1280,128]{1,0:T(8,128)(2,1)S(1)} all-gather(bf16[80,128]{1,0:T(8,128)(2,1)S(1)} %shard_map.143), channel_id=3, replica_groups=mesh['ep_0'=8,'ep_1'=2,'ep_2'=2,'tp_0'=4,'tp_1'=4] {'ep_0','ep_2'}, dimensions={0}, use_global_device_ids=true | all-gather | bytes 348160 | tf_op jit(solution)/shard_map/all_gather | solution.py:398
  71.2 2.9 %shard_map.144 = (bf16[256,128]{1,0:T(8,128)(2,1)S(1)}, bf16[4,384,128]{2,1,0:T(8,128)(2,1)}, bf16[4,384,128]{2,1,0:T(8,128)(2,1)}) custom-call(s32[1]{0:T(128)} %bitcast.5.place, s32[1]{0:T(128)} %bitcast.6.group, s32[1]{0:T(128)} %bitcast.lane, bf16[16,80,128]{2,1,0:T(8,128)(2,1)S(1)} %bitcast.16, bf16[4,144,128]{2,1,0:T(8,128)(2,1)S(1)} %bitcast.15, ...), custom_call_target="tpu_custom_call" | custom-call | tf_op jit(solution)/shard_map/pallas_call | solution.py:50
  74.1 4.2 %shard_map.145 = bf16[4,1280,128]{2,1,0:T(8,128)(2,1)} custom-call(bf16[16,512,128]{2,1,0:T(8,128)(2,1)S(1)} %all-to-all-done.1.rows, bf16[256,128]{1,0:T(8,128)(2,1)S(1)} %get-tuple-element.21.heads, bf16[1,2048,256]{2,1,0:T(8,128)(2,1)} %w_gate.1, bf16[1,2048,256]{2,1,0:T(8,128)(2,1)} %w_up.1), custom_call_target="tpu_custom_call" | custom-call | tf_op jit(solution)/shard_map/pallas_call | solution.py:50
  78.4 4.4 %all-to-all-start.2 = ((bf16[4,1280,128]{2,1,0:T(8,128)(2,1)}), bf16[4,1280,128]{2,1,0:T(8,128)(2,1)S(1)}, u32[]{:S(2)}, u32[]{:S(2)}) async-start(bf16[4,1280,128]{2,1,0:T(8,128)(2,1)} %shard_map.145), calls=%async_computation.2 | async-start | bytes 2621440 | tf_op jit(solution)/shard_map/all_to_all | solution.py:524
  82.8 2.5 %collective-permute-start = (bf16[4,384,128]{2,1,0:T(8,128)(2,1)S(1)}, bf16[4,384,128]{2,1,0:T(8,128)(2,1)S(1)}, u32[]{:S(2)}, u32[]{:S(2)}) collective-permute-start(bf16[4,384,128]{2,1,0:T(8,128)(2,1)S(1)} %copy-done.3), channel_id=1, source_target_pairs={{0,1},{1,2},{2,3},{3,0},{4,5},{5,6},{6,7},{7,4},{8,9},{9,10},{10,1... | collective-permute-start | bytes 1179656 | tf_op jit(solution)/shard_map/ppermute | solution.py:439
  86.2 4.2 %collective-permute-start.1 = (bf16[4,384,128]{2,1,0:T(8,128)(2,1)S(1)}, bf16[4,384,128]{2,1,0:T(8,128)(2,1)S(1)}, u32[]{:S(2)}, u32[]{:S(2)}) collective-permute-start(bf16[4,384,128]{2,1,0:T(8,128)(2,1)S(1)} %shard_map.146), channel_id=1, source_target_pairs={{0,2},{1,3},{2,0},{3,1},{4,6},{5,7},{6,4},{7,5},{8,10},{9,11},{10,... | collective-permute-start | bytes 1179656 | tf_op jit(solution)/shard_map/ppermute | solution.py:439
  90.5 1.9 %collective-permute-start.2 = (bf16[4,384,128]{2,1,0:T(8,128)(2,1)S(1)}, bf16[4,384,128]{2,1,0:T(8,128)(2,1)S(1)}, u32[]{:S(2)}, u32[]{:S(2)}) collective-permute-start(bf16[4,384,128]{2,1,0:T(8,128)(2,1)S(1)} %copy-done.2), channel_id=1, source_target_pairs={{0,3},{1,0},{2,1},{3,2},{4,7},{5,4},{6,5},{7,6},{8,11},{9,8},{10,9... | collective-permute-start | bytes 1179656 | tf_op jit(solution)/shard_map/ppermute | solution.py:439
  92.4 4.2 %collective-permute-done.w_1 = bf16[4,384,128]{2,1,0:T(8,128)(2,1)S(1)} collective-permute-done((bf16[4,384,128]{2,1,0:T(8,128)(2,1)S(1)}, bf16[4,384,128]{2,1,0:T(8,128)(2,1)S(1)}, u32[]{:S(2)}, u32[]{:S(2)}) %collective-permute-start) | collective-permute-done | bytes 393248 | tf_op jit(solution)/shard_map/ppermute | solution.py:439
  96.6 5.0 %collective-permute-done.1.w_2 = bf16[4,384,128]{2,1,0:T(8,128)(2,1)S(1)} collective-permute-done((bf16[4,384,128]{2,1,0:T(8,128)(2,1)S(1)}, bf16[4,384,128]{2,1,0:T(8,128)(2,1)S(1)}, u32[]{:S(2)}, u32[]{:S(2)}) %collective-permute-start.1) | collective-permute-done | bytes 393248 | tf_op jit(solution)/shard_map/ppermute | solution.py:439
  101.7 7.2 %collective-permute-done.2.w_3 = bf16[4,384,128]{2,1,0:T(8,128)(2,1)S(1)} collective-permute-done((bf16[4,384,128]{2,1,0:T(8,128)(2,1)S(1)}, bf16[4,384,128]{2,1,0:T(8,128)(2,1)S(1)}, u32[]{:S(2)}, u32[]{:S(2)}) %collective-permute-start.2) | collective-permute-done | bytes 393248 | tf_op jit(solution)/shard_map/ppermute | solution.py:439
  108.9 2.1 %shard_map.147 = (bf16[4,512,128]{2,1,0:T(8,128)(2,1)S(1)}, bf16[256,128]{1,0:T(8,128)(2,1)S(1)}, bf16[256,128]{1,0:T(8,128)(2,1)S(1)}, bf16[256,128]{1,0:T(8,128)(2,1)S(1)}, bf16[256,128]{1,0:T(8,128)(2,1)S(1)}) custom-call(s32[1]{0:T(128)} %bitcast.lane, bf16[4,1280,128]{2,1,0:T(8,128)(2,1)S(1)} %all-to-all-done.2.got, bf16[4,4,256,128]{3,2,1,0:T(8,128)(2,1)} %bitcast.21, ...), custom_call_target="tpu_custom_call" | custom-call | tf_op jit(solution)/shard_map/pallas_call | solution.py:50
  111.0 11.9 %all_to_all.26.parts = bf16[4,512,128]{2,1,0:T(8,128)(2,1)S(1)} all-to-all(bf16[4,512,128]{2,1,0:T(8,128)(2,1)S(1)} %get-tuple-element.28), channel_id=1, replica_groups=mesh['ep_0'=8,'ep_1'=2,'ep_2'=2,'tp_0'=4,'tp_1'=4] {'tp_1'}, dimensions={0} | all-to-all | bytes 1048576 | tf_op jit(solution)/shard_map/all_to_all | solution.py:535
  123.6 6.1 %all-to-all-start.4 = ((bf16[32,16,128]{2,1,0:T(8,128)(2,1)}), bf16[32,16,128]{2,1,0:T(8,128)(2,1)S(1)}, u32[]{:S(2)}, u32[]{:S(2)}) async-start(bf16[32,16,128]{2,1,0:T(8,128)(2,1)} %shard_map.149), calls=%async_computation.4 | async-start | bytes 262144 | tf_op jit(solution)/shard_map/all_to_all | solution.py:537
  129.7 2.1 %collective-permute-start.3 = (bf16[256,128]{1,0:T(8,128)(2,1)S(1)}, bf16[256,128]{1,0:T(8,128)(2,1)S(1)}, u32[]{:S(2)}, u32[]{:S(2)}) collective-permute-start(bf16[256,128]{1,0:T(8,128)(2,1)S(1)} %get-tuple-element.25), channel_id=1, source_target_pairs={{0,3},{1,0},{2,1},{3,2},{4,7},{5,4},{6,5},{7,6},{8,11},{9,8},{10,9... | collective-permute-start | bytes 196616 | tf_op jit(solution)/shard_map/ppermute | solution.py:439
  131.9 5.2 %collective-permute-start.4 = (bf16[256,128]{1,0:T(8,128)(2,1)S(1)}, bf16[256,128]{1,0:T(8,128)(2,1)S(1)}, u32[]{:S(2)}, u32[]{:S(2)}) collective-permute-start(bf16[256,128]{1,0:T(8,128)(2,1)S(1)} %get-tuple-element.26), channel_id=1, source_target_pairs={{0,2},{1,3},{2,0},{3,1},{4,6},{5,7},{6,4},{7,5},{8,10},{9,11},{10,... | collective-permute-start | bytes 196616 | tf_op jit(solution)/shard_map/ppermute | solution.py:439
  137.1 3.1 %collective-permute-start.5 = (bf16[256,128]{1,0:T(8,128)(2,1)S(1)}, bf16[256,128]{1,0:T(8,128)(2,1)S(1)}, u32[]{:S(2)}, u32[]{:S(2)}) collective-permute-start(bf16[256,128]{1,0:T(8,128)(2,1)S(1)} %get-tuple-element.27), channel_id=1, source_target_pairs={{0,1},{1,2},{2,3},{3,0},{4,5},{5,6},{6,7},{7,4},{8,9},{9,10},{10,1... | collective-permute-start | bytes 196616 | tf_op jit(solution)/shard_map/ppermute | solution.py:439
  140.5 2.8 %collective-permute-done.5.p_3 = bf16[256,128]{1,0:T(8,128)(2,1)S(1)} collective-permute-done((bf16[256,128]{1,0:T(8,128)(2,1)S(1)}, bf16[256,128]{1,0:T(8,128)(2,1)S(1)}, u32[]{:S(2)}, u32[]{:S(2)}) %collective-permute-start.5) | collective-permute-done | bytes 65568 | tf_op jit(solution)/shard_map/ppermute | solution.py:439
  143.9 3.0 %all-to-all-done.4.back = bf16[32,16,128]{2,1,0:T(8,128)(2,1)S(1)} async-done(((bf16[32,16,128]{2,1,0:T(8,128)(2,1)}), bf16[32,16,128]{2,1,0:T(8,128)(2,1)S(1)}, u32[]{:S(2)}, u32[]{:S(2)}) %all-to-all-start.4) | async-done | bytes 131104 | tf_op jit(solution)/shard_map/all_to_all | solution.py:537
  (23 shorter events, 4.3 us)
Async XLA Ops:
  37.2 34.0 %copy-start = (bf16[256,128]{1,0:T(8,128)(2,1)S(1)}, bf16[256,128]{1,0:T(8,128)(2,1)}, u32[]{:S(2)}) copy-start(bf16[256,128]{1,0:T(8,128)(2,1)} %gates.1) | copy-start | bytes 196612
  37.2 36.9 %all-to-all-start.1 = ((bf16[16,512,128]{2,1,0:T(8,128)(2,1)}), bf16[16,512,128]{2,1,0:T(8,128)(2,1)S(1)}, u32[]{:S(2)}, u32[]{:S(2)}) async-start(bf16[16,512,128]{2,1,0:T(8,128)(2,1)} %shard_map.141), calls=%async_computation.1 | async-start | bytes 4194304 | tf_op jit(solution)/shard_map/all_to_all | solution.py:501
  78.4 4.4 %copy-start.3 = (bf16[4,384,128]{2,1,0:T(8,128)(2,1)S(1)}, bf16[4,384,128]{2,1,0:T(8,128)(2,1)}, u32[]{:S(2)}) copy-start(bf16[4,384,128]{2,1,0:T(8,128)(2,1)} %get-tuple-element.22) | copy-start | bytes 1179652
  78.4 12.1 %copy-start.2 = (bf16[4,384,128]{2,1,0:T(8,128)(2,1)S(1)}, bf16[4,384,128]{2,1,0:T(8,128)(2,1)}, u32[]{:S(2)}) copy-start(bf16[4,384,128]{2,1,0:T(8,128)(2,1)} %get-tuple-element.23) | copy-start | bytes 1179652
  78.4 30.5 %all-to-all-start.2 = ((bf16[4,1280,128]{2,1,0:T(8,128)(2,1)}), bf16[4,1280,128]{2,1,0:T(8,128)(2,1)S(1)}, u32[]{:S(2)}, u32[]{:S(2)}) async-start(bf16[4,1280,128]{2,1,0:T(8,128)(2,1)} %shard_map.145), calls=%async_computation.2 | async-start | bytes 2621440 | tf_op jit(solution)/shard_map/all_to_all | solution.py:524
  82.8 13.9 %collective-permute-start = (bf16[4,384,128]{2,1,0:T(8,128)(2,1)S(1)}, bf16[4,384,128]{2,1,0:T(8,128)(2,1)S(1)}, u32[]{:S(2)}, u32[]{:S(2)}) collective-permute-start(bf16[4,384,128]{2,1,0:T(8,128)(2,1)S(1)} %copy-done.3), channel_id=1, source_target_pairs={{0,1},{1,2},{2,3},{3,0},{4,5},{5,6},{6,7},{7,4},{8,9},{9,10},{10,1... | collective-permute-start | bytes 1179656 | tf_op jit(solution)/shard_map/ppermute | solution.py:439
  86.2 15.4 %collective-permute-start.1 = (bf16[4,384,128]{2,1,0:T(8,128)(2,1)S(1)}, bf16[4,384,128]{2,1,0:T(8,128)(2,1)S(1)}, u32[]{:S(2)}, u32[]{:S(2)}) collective-permute-start(bf16[4,384,128]{2,1,0:T(8,128)(2,1)S(1)} %shard_map.146), channel_id=1, source_target_pairs={{0,2},{1,3},{2,0},{3,1},{4,6},{5,7},{6,4},{7,5},{8,10},{9,11},{10,... | collective-permute-start | bytes 1179656 | tf_op jit(solution)/shard_map/ppermute | solution.py:439
  90.5 49.8 %copy-start.1 = (f32[256,2]{0,1:T(2,128)S(1)}, f32[256,2]{0,1:T(2,128)}, u32[]{:S(2)}) copy-start(f32[256,2]{0,1:T(2,128)} %param.22) | copy-start | bytes 6148
  90.5 18.4 %collective-permute-start.2 = (bf16[4,384,128]{2,1,0:T(8,128)(2,1)S(1)}, bf16[4,384,128]{2,1,0:T(8,128)(2,1)S(1)}, u32[]{:S(2)}, u32[]{:S(2)}) collective-permute-start(bf16[4,384,128]{2,1,0:T(8,128)(2,1)S(1)} %copy-done.2), channel_id=1, source_target_pairs={{0,3},{1,0},{2,1},{3,2},{4,7},{5,4},{6,5},{7,6},{8,11},{9,8},{10,9... | collective-permute-start | bytes 1179656 | tf_op jit(solution)/shard_map/ppermute | solution.py:439
  123.6 23.3 %all-to-all-start.4 = ((bf16[32,16,128]{2,1,0:T(8,128)(2,1)}), bf16[32,16,128]{2,1,0:T(8,128)(2,1)S(1)}, u32[]{:S(2)}, u32[]{:S(2)}) async-start(bf16[32,16,128]{2,1,0:T(8,128)(2,1)} %shard_map.149), calls=%async_computation.4 | async-start | bytes 262144 | tf_op jit(solution)/shard_map/all_to_all | solution.py:537
  129.7 10.7 %collective-permute-start.3 = (bf16[256,128]{1,0:T(8,128)(2,1)S(1)}, bf16[256,128]{1,0:T(8,128)(2,1)S(1)}, u32[]{:S(2)}, u32[]{:S(2)}) collective-permute-start(bf16[256,128]{1,0:T(8,128)(2,1)S(1)} %get-tuple-element.25), channel_id=1, source_target_pairs={{0,3},{1,0},{2,1},{3,2},{4,7},{5,4},{6,5},{7,6},{8,11},{9,8},{10,9... | collective-permute-start | bytes 196616 | tf_op jit(solution)/shard_map/ppermute | solution.py:439
  131.9 8.6 %collective-permute-start.4 = (bf16[256,128]{1,0:T(8,128)(2,1)S(1)}, bf16[256,128]{1,0:T(8,128)(2,1)S(1)}, u32[]{:S(2)}, u32[]{:S(2)}) collective-permute-start(bf16[256,128]{1,0:T(8,128)(2,1)S(1)} %get-tuple-element.26), channel_id=1, source_target_pairs={{0,2},{1,3},{2,0},{3,1},{4,6},{5,7},{6,4},{7,5},{8,10},{9,11},{10,... | collective-permute-start | bytes 196616 | tf_op jit(solution)/shard_map/ppermute | solution.py:439
  137.1 6.2 %collective-permute-start.5 = (bf16[256,128]{1,0:T(8,128)(2,1)S(1)}, bf16[256,128]{1,0:T(8,128)(2,1)S(1)}, u32[]{:S(2)}, u32[]{:S(2)}) collective-permute-start(bf16[256,128]{1,0:T(8,128)(2,1)S(1)} %get-tuple-element.27), channel_id=1, source_target_pairs={{0,1},{1,2},{2,3},{3,0},{4,5},{5,6},{6,7},{7,4},{8,9},{9,10},{10,1... | collective-permute-start | bytes 196616 | tf_op jit(solution)/shard_map/ppermute | solution.py:439

commit v5 on v4

--- a/solution.py
+++ b/solution.py
@@ -158,18 +158,21 @@
     per = parts // chunks
     half = count // 2
     final = []
+
+    def product(side, kind, near_w):
+        total = jnp.zeros((half, w_gate.shape[2]), F32)
+        for k in range(chunks):
+            if side == 0:
+                copies[k][kind].wait()
+            span = slice(side * half, (side + 1) * half)
+            left = jnp.concatenate([rows[k * per + j, span, :] for j in range(per)], axis=1)
+            total += dot(left, near_w[k * tall : (k + 1) * tall, :])
+        return total
+
+    gates = [product(side, 0, near_gate) for side in range(2)]
     for side in range(2):
-        span = slice(side * half, (side + 1) * half)
-        sums = []
-        for kind, near_w in ((0, near_gate), (1, near_up)):
-            total = jnp.zeros((half, w_gate.shape[2]), F32)
-            for k in range(chunks):
-                if side == 0:
-                    copies[k][kind].wait()
-                left = jnp.concatenate([rows[k * per + j, span, :] for j in range(per)], axis=1)
-                total += dot(left, near_w[k * tall : (k + 1) * tall, :])
-            sums.append(total)
-        gate, up = sums
+        gate = gates[side]
+        up = product(side, 1, near_up)
         hidden = (gate / (1.0 + jnp.exp(-gate)) * up).astype(BF)
         for part in range(2):
             at = part * count + side * half

time: 150 us -> 150 us (level)
  no operation moved by 1% of the time
where the time goes in v5:
time: 150 us; the launch traced here: 148 us
  blocking collectives  67.6 us (45%)
  starting transfers between devices  37.1 us (25%)
  waiting for transfers between devices  22.2 us (15%)
  Pallas kernels  19 us (13%)
    all_to_all x1, blocking collectives, both_halves(): arrived = lax.all_to_all(send, EP, 0, 0, tiled=True)  32.5 us
    ppermute x6, waiting for transfers between devices, shifted(): lax.ppermute(array, axis, [(k, (k + far) % peers) for k in range(peers)])  19.2 us
    ppermute x6, starting transfers between devices, shifted(): lax.ppermute(array, axis, [(k, (k + far) % peers) for k in range(peers)])  19 us
    pallas_call x11, Pallas kernels, call(): pl.pallas_call(body, in_specs=[places[kind] for kind in kinds], out_specs...  19 us
    all_gather x1, blocking collectives, retention_heads(): far = lax.all_gather(pay, ('ep_0', 'ep_2'))  17.8 us
    all_to_all x1, blocking collectives, both_halves(): pieces = lax.all_to_all(partial, 'tp_1', 0, 0, tiled=True)  11.9 us
    all_to_all x1, starting transfers between devices, both_halves(): rows = lax.all_to_all(spread, TP, 0, 0, tiled=True)  7.57 us
    all_to_all x1, starting transfers between devices, both_halves(): back = lax.all_to_all(summed, EP, 0, 0, tiled=True)  6.09 us
  transfers between devices with their start and end apart: 9, of which 5 were waited for; matrix products, arithmetic and copies ran while one was open for 1% of the time, Pallas kernels for 5%

profile of v5, /device:TPU:6, one launch (start us, length us, event | category | flops | bytes accessed | tf_op | source)
XLA Modules:
  0.0 147.7 jit_solution(3493849248144983982)
XLA Ops:
  0.6 2.6 %shard_map.140 = (bf16[32,16,128]{2,1,0:T(8,128)(2,1)S(1)}, s32[2,256]{1,0:T(2,128)S(1)}) custom-call(s32[1]{0:T(128)} %bitcast.1.turn, s32[2,256]{1,0:T(2,128)} %bitcast.26, bf16[16,128]{1,0:T(8,128)(2,1)} %bitcast.25, bf16[256,2048]{1,0:T(8,128)(2,1)} %source.1), custom_call_target="tpu_custom_call" | custom-call | tf_op jit(solution)/shard_map/pallas_call | solution.py:50
  3.2 32.5 %all_to_all.25 = bf16[32,16,128]{2,1,0:T(8,128)(2,1)S(1)} all-to-all(bf16[32,16,128]{2,1,0:T(8,128)(2,1)S(1)} %get-tuple-element.17), channel_id=1, replica_groups=mesh['ep_0'=8,'ep_1'=2,'ep_2'=2,'tp_0'=4,'tp_1'=4] {'ep_0','ep_1','ep_2'}, dimensions={0} | all-to-all | bytes 262144 | tf_op jit(solution)/shard_map/all_to_all | solution.py:495
  35.7 1.5 shard_map.141
  37.2 7.6 %all-to-all-start.1 = ((bf16[16,512,128]{2,1,0:T(8,128)(2,1)}), bf16[16,512,128]{2,1,0:T(8,128)(2,1)S(1)}, u32[]{:S(2)}, u32[]{:S(2)}) async-start(bf16[16,512,128]{2,1,0:T(8,128)(2,1)} %shard_map.141), calls=%async_computation.1 | async-start | bytes 4194304 | tf_op jit(solution)/shard_map/all_to_all | solution.py:504
  45.4 2.5 %shard_map.142 = (f32[256,128]{1,0:T(8,128)}, f32[256,128]{1,0:T(8,128)}, bf16[144,128]{1,0:T(8,128)(2,1)S(1)}) custom-call(bf16[256,128]{1,0:T(8,128)(2,1)} %q.1, bf16[256,128]{1,0:T(8,128)(2,1)} %k.1, bf16[256,128]{1,0:T(8,128)(2,1)} %v.1, f32[2,128]{1,0:T(2,128)} %bitcast.27, f32[256,128]{1,0:T(8,128)S(1)} %get-tuple-element.33.cosine, ...), custom_call_target="tpu_custom_call" | custom-call | tf_op jit(solution)/shard_map/pallas_call | solution.py:50
  47.9 5.4 %all-gather = bf16[576,128]{1,0:T(8,128)(2,1)S(1)} all-gather(bf16[144,128]{1,0:T(8,128)(2,1)S(1)} %get-tuple-element.18), channel_id=2, replica_groups=mesh['ep_0'=8,'ep_1'=2,'ep_2'=2,'tp_0'=4,'tp_1'=4] {'ep_1','ep_2'}, dimensions={0}, use_global_device_ids=true | all-gather | bytes 184320 | tf_op jit(solution)/shard_map/all_gather | solution.py:392
  53.4 17.8 %all-gather.1 = bf16[1280,128]{1,0:T(8,128)(2,1)S(1)} all-gather(bf16[80,128]{1,0:T(8,128)(2,1)S(1)} %shard_map.143), channel_id=3, replica_groups=mesh['ep_0'=8,'ep_1'=2,'ep_2'=2,'tp_0'=4,'tp_1'=4] {'ep_0','ep_2'}, dimensions={0}, use_global_device_ids=true | all-gather | bytes 348160 | tf_op jit(solution)/shard_map/all_gather | solution.py:401
  71.2 2.9 %shard_map.144 = (bf16[256,128]{1,0:T(8,128)(2,1)S(1)}, bf16[4,384,128]{2,1,0:T(8,128)(2,1)}, bf16[4,384,128]{2,1,0:T(8,128)(2,1)}) custom-call(s32[1]{0:T(128)} %bitcast.5.place, s32[1]{0:T(128)} %bitcast.6.group, s32[1]{0:T(128)} %bitcast.lane, bf16[16,80,128]{2,1,0:T(8,128)(2,1)S(1)} %bitcast.16, bf16[4,144,128]{2,1,0:T(8,128)(2,1)S(1)} %bitcast.15, ...), custom_call_target="tpu_custom_call" | custom-call | tf_op jit(solution)/shard_map/pallas_call | solution.py:50
  74.1 4.0 %shard_map.145 = bf16[4,1280,128]{2,1,0:T(8,128)(2,1)} custom-call(bf16[16,512,128]{2,1,0:T(8,128)(2,1)S(1)} %all-to-all-done.1.rows, bf16[256,128]{1,0:T(8,128)(2,1)S(1)} %get-tuple-element.21.heads, bf16[1,2048,256]{2,1,0:T(8,128)(2,1)} %w_gate.1, bf16[1,2048,256]{2,1,0:T(8,128)(2,1)} %w_up.1), custom_call_target="tpu_custom_call" | custom-call | tf_op jit(solution)/shard_map/pallas_call | solution.py:50
  78.1 4.4 %all-to-all-start.2 = ((bf16[4,1280,128]{2,1,0:T(8,128)(2,1)}), bf16[4,1280,128]{2,1,0:T(8,128)(2,1)S(1)}, u32[]{:S(2)}, u32[]{:S(2)}) async-start(bf16[4,1280,128]{2,1,0:T(8,128)(2,1)} %shard_map.145), calls=%async_computation.2 | async-start | bytes 2621440 | tf_op jit(solution)/shard_map/all_to_all | solution.py:527
  82.5 2.5 %collective-permute-start = (bf16[4,384,128]{2,1,0:T(8,128)(2,1)S(1)}, bf16[4,384,128]{2,1,0:T(8,128)(2,1)S(1)}, u32[]{:S(2)}, u32[]{:S(2)}) collective-permute-start(bf16[4,384,128]{2,1,0:T(8,128)(2,1)S(1)} %copy-done.3), channel_id=1, source_target_pairs={{0,1},{1,2},{2,3},{3,0},{4,5},{5,6},{6,7},{7,4},{8,9},{9,10},{10,1... | collective-permute-start | bytes 1179656 | tf_op jit(solution)/shard_map/ppermute | solution.py:442
  86.0 4.2 %collective-permute-start.1 = (bf16[4,384,128]{2,1,0:T(8,128)(2,1)S(1)}, bf16[4,384,128]{2,1,0:T(8,128)(2,1)S(1)}, u32[]{:S(2)}, u32[]{:S(2)}) collective-permute-start(bf16[4,384,128]{2,1,0:T(8,128)(2,1)S(1)} %shard_map.146), channel_id=1, source_target_pairs={{0,2},{1,3},{2,0},{3,1},{4,6},{5,7},{6,4},{7,5},{8,10},{9,11},{10,... | collective-permute-start | bytes 1179656 | tf_op jit(solution)/shard_map/ppermute | solution.py:442
  90.3 1.9 %collective-permute-start.2 = (bf16[4,384,128]{2,1,0:T(8,128)(2,1)S(1)}, bf16[4,384,128]{2,1,0:T(8,128)(2,1)S(1)}, u32[]{:S(2)}, u32[]{:S(2)}) collective-permute-start(bf16[4,384,128]{2,1,0:T(8,128)(2,1)S(1)} %copy-done.2), channel_id=1, source_target_pairs={{0,3},{1,0},{2,1},{3,2},{4,7},{5,4},{6,5},{7,6},{8,11},{9,8},{10,9... | collective-permute-start | bytes 1179656 | tf_op jit(solution)/shard_map/ppermute | solution.py:442
  92.2 4.2 %collective-permute-done.w_1 = bf16[4,384,128]{2,1,0:T(8,128)(2,1)S(1)} collective-permute-done((bf16[4,384,128]{2,1,0:T(8,128)(2,1)S(1)}, bf16[4,384,128]{2,1,0:T(8,128)(2,1)S(1)}, u32[]{:S(2)}, u32[]{:S(2)}) %collective-permute-start) | collective-permute-done | bytes 393248 | tf_op jit(solution)/shard_map/ppermute | solution.py:442
  96.4 5.0 %collective-permute-done.1.w_2 = bf16[4,384,128]{2,1,0:T(8,128)(2,1)S(1)} collective-permute-done((bf16[4,384,128]{2,1,0:T(8,128)(2,1)S(1)}, bf16[4,384,128]{2,1,0:T(8,128)(2,1)S(1)}, u32[]{:S(2)}, u32[]{:S(2)}) %collective-permute-start.1) | collective-permute-done | bytes 393248 | tf_op jit(solution)/shard_map/ppermute | solution.py:442
  101.4 7.2 %collective-permute-done.2.w_3 = bf16[4,384,128]{2,1,0:T(8,128)(2,1)S(1)} collective-permute-done((bf16[4,384,128]{2,1,0:T(8,128)(2,1)S(1)}, bf16[4,384,128]{2,1,0:T(8,128)(2,1)S(1)}, u32[]{:S(2)}, u32[]{:S(2)}) %collective-permute-start.2) | collective-permute-done | bytes 393248 | tf_op jit(solution)/shard_map/ppermute | solution.py:442
  108.6 2.1 %shard_map.147 = (bf16[4,512,128]{2,1,0:T(8,128)(2,1)S(1)}, bf16[256,128]{1,0:T(8,128)(2,1)S(1)}, bf16[256,128]{1,0:T(8,128)(2,1)S(1)}, bf16[256,128]{1,0:T(8,128)(2,1)S(1)}, bf16[256,128]{1,0:T(8,128)(2,1)S(1)}) custom-call(s32[1]{0:T(128)} %bitcast.lane, bf16[4,1280,128]{2,1,0:T(8,128)(2,1)S(1)} %all-to-all-done.2.got, bf16[4,4,256,128]{3,2,1,0:T(8,128)(2,1)} %bitcast.21, ...), custom_call_target="tpu_custom_call" | custom-call | tf_op jit(solution)/shard_map/pallas_call | solution.py:50
  110.8 11.9 %all_to_all.26.parts = bf16[4,512,128]{2,1,0:T(8,128)(2,1)S(1)} all-to-all(bf16[4,512,128]{2,1,0:T(8,128)(2,1)S(1)} %get-tuple-element.28), channel_id=1, replica_groups=mesh['ep_0'=8,'ep_1'=2,'ep_2'=2,'tp_0'=4,'tp_1'=4] {'tp_1'}, dimensions={0} | all-to-all | bytes 1048576 | tf_op jit(solution)/shard_map/all_to_all | solution.py:538
  123.4 6.1 %all-to-all-start.4 = ((bf16[32,16,128]{2,1,0:T(8,128)(2,1)}), bf16[32,16,128]{2,1,0:T(8,128)(2,1)S(1)}, u32[]{:S(2)}, u32[]{:S(2)}) async-start(bf16[32,16,128]{2,1,0:T(8,128)(2,1)} %shard_map.149), calls=%async_computation.4 | async-start | bytes 262144 | tf_op jit(solution)/shard_map/all_to_all | solution.py:540
  129.5 2.1 %collective-permute-start.3 = (bf16[256,128]{1,0:T(8,128)(2,1)S(1)}, bf16[256,128]{1,0:T(8,128)(2,1)S(1)}, u32[]{:S(2)}, u32[]{:S(2)}) collective-permute-start(bf16[256,128]{1,0:T(8,128)(2,1)S(1)} %get-tuple-element.25), channel_id=1, source_target_pairs={{0,3},{1,0},{2,1},{3,2},{4,7},{5,4},{6,5},{7,6},{8,11},{9,8},{10,9... | collective-permute-start | bytes 196616 | tf_op jit(solution)/shard_map/ppermute | solution.py:442
  131.6 5.2 %collective-permute-start.4 = (bf16[256,128]{1,0:T(8,128)(2,1)S(1)}, bf16[256,128]{1,0:T(8,128)(2,1)S(1)}, u32[]{:S(2)}, u32[]{:S(2)}) collective-permute-start(bf16[256,128]{1,0:T(8,128)(2,1)S(1)} %get-tuple-element.26), channel_id=1, source_target_pairs={{0,2},{1,3},{2,0},{3,1},{4,6},{5,7},{6,4},{7,5},{8,10},{9,11},{10,... | collective-permute-start | bytes 196616 | tf_op jit(solution)/shard_map/ppermute | solution.py:442
  136.9 3.1 %collective-permute-start.5 = (bf16[256,128]{1,0:T(8,128)(2,1)S(1)}, bf16[256,128]{1,0:T(8,128)(2,1)S(1)}, u32[]{:S(2)}, u32[]{:S(2)}) collective-permute-start(bf16[256,128]{1,0:T(8,128)(2,1)S(1)} %get-tuple-element.27), channel_id=1, source_target_pairs={{0,1},{1,2},{2,3},{3,0},{4,5},{5,6},{6,7},{7,4},{8,9},{9,10},{10,1... | collective-permute-start | bytes 196616 | tf_op jit(solution)/shard_map/ppermute | solution.py:442
  140.3 2.8 %collective-permute-done.5.p_3 = bf16[256,128]{1,0:T(8,128)(2,1)S(1)} collective-permute-done((bf16[256,128]{1,0:T(8,128)(2,1)S(1)}, bf16[256,128]{1,0:T(8,128)(2,1)S(1)}, u32[]{:S(2)}, u32[]{:S(2)}) %collective-permute-start.5) | collective-permute-done | bytes 65568 | tf_op jit(solution)/shard_map/ppermute | solution.py:442
  143.7 3.0 %all-to-all-done.4.back = bf16[32,16,128]{2,1,0:T(8,128)(2,1)S(1)} async-done(((bf16[32,16,128]{2,1,0:T(8,128)(2,1)}), bf16[32,16,128]{2,1,0:T(8,128)(2,1)S(1)}, u32[]{:S(2)}, u32[]{:S(2)}) %all-to-all-start.4) | async-done | bytes 131104 | tf_op jit(solution)/shard_map/all_to_all | solution.py:540
  (23 shorter events, 4.3 us)
Async XLA Ops:
  37.2 34.0 %copy-start = (bf16[256,128]{1,0:T(8,128)(2,1)S(1)}, bf16[256,128]{1,0:T(8,128)(2,1)}, u32[]{:S(2)}) copy-start(bf16[256,128]{1,0:T(8,128)(2,1)} %gates.1) | copy-start | bytes 196612
  37.2 36.9 %all-to-all-start.1 = ((bf16[16,512,128]{2,1,0:T(8,128)(2,1)}), bf16[16,512,128]{2,1,0:T(8,128)(2,1)S(1)}, u32[]{:S(2)}, u32[]{:S(2)}) async-start(bf16[16,512,128]{2,1,0:T(8,128)(2,1)} %shard_map.141), calls=%async_computation.1 | async-start | bytes 4194304 | tf_op jit(solution)/shard_map/all_to_all | solution.py:504
  78.1 4.4 %copy-start.3 = (bf16[4,384,128]{2,1,0:T(8,128)(2,1)S(1)}, bf16[4,384,128]{2,1,0:T(8,128)(2,1)}, u32[]{:S(2)}) copy-start(bf16[4,384,128]{2,1,0:T(8,128)(2,1)} %get-tuple-element.22) | copy-start | bytes 1179652
  78.1 12.1 %copy-start.2 = (bf16[4,384,128]{2,1,0:T(8,128)(2,1)S(1)}, bf16[4,384,128]{2,1,0:T(8,128)(2,1)}, u32[]{:S(2)}) copy-start(bf16[4,384,128]{2,1,0:T(8,128)(2,1)} %get-tuple-element.23) | copy-start | bytes 1179652
  78.1 30.5 %all-to-all-start.2 = ((bf16[4,1280,128]{2,1,0:T(8,128)(2,1)}), bf16[4,1280,128]{2,1,0:T(8,128)(2,1)S(1)}, u32[]{:S(2)}, u32[]{:S(2)}) async-start(bf16[4,1280,128]{2,1,0:T(8,128)(2,1)} %shard_map.145), calls=%async_computation.2 | async-start | bytes 2621440 | tf_op jit(solution)/shard_map/all_to_all | solution.py:527
  82.5 13.9 %collective-permute-start = (bf16[4,384,128]{2,1,0:T(8,128)(2,1)S(1)}, bf16[4,384,128]{2,1,0:T(8,128)(2,1)S(1)}, u32[]{:S(2)}, u32[]{:S(2)}) collective-permute-start(bf16[4,384,128]{2,1,0:T(8,128)(2,1)S(1)} %copy-done.3), channel_id=1, source_target_pairs={{0,1},{1,2},{2,3},{3,0},{4,5},{5,6},{6,7},{7,4},{8,9},{9,10},{10,1... | collective-permute-start | bytes 1179656 | tf_op jit(solution)/shard_map/ppermute | solution.py:442
  86.0 15.4 %collective-permute-start.1 = (bf16[4,384,128]{2,1,0:T(8,128)(2,1)S(1)}, bf16[4,384,128]{2,1,0:T(8,128)(2,1)S(1)}, u32[]{:S(2)}, u32[]{:S(2)}) collective-permute-start(bf16[4,384,128]{2,1,0:T(8,128)(2,1)S(1)} %shard_map.146), channel_id=1, source_target_pairs={{0,2},{1,3},{2,0},{3,1},{4,6},{5,7},{6,4},{7,5},{8,10},{9,11},{10,... | collective-permute-start | bytes 1179656 | tf_op jit(solution)/shard_map/ppermute | solution.py:442
  90.2 49.8 %copy-start.1 = (f32[256,2]{0,1:T(2,128)S(1)}, f32[256,2]{0,1:T(2,128)}, u32[]{:S(2)}) copy-start(f32[256,2]{0,1:T(2,128)} %param.22) | copy-start | bytes 6148
  90.3 18.4 %collective-permute-start.2 = (bf16[4,384,128]{2,1,0:T(8,128)(2,1)S(1)}, bf16[4,384,128]{2,1,0:T(8,128)(2,1)S(1)}, u32[]{:S(2)}, u32[]{:S(2)}) collective-permute-start(bf16[4,384,128]{2,1,0:T(8,128)(2,1)S(1)} %copy-done.2), channel_id=1, source_target_pairs={{0,3},{1,0},{2,1},{3,2},{4,7},{5,4},{6,5},{7,6},{8,11},{9,8},{10,9... | collective-permute-start | bytes 1179656 | tf_op jit(solution)/shard_map/ppermute | solution.py:442
  123.4 23.3 %all-to-all-start.4 = ((bf16[32,16,128]{2,1,0:T(8,128)(2,1)}), bf16[32,16,128]{2,1,0:T(8,128)(2,1)S(1)}, u32[]{:S(2)}, u32[]{:S(2)}) async-start(bf16[32,16,128]{2,1,0:T(8,128)(2,1)} %shard_map.149), calls=%async_computation.4 | async-start | bytes 262144 | tf_op jit(solution)/shard_map/all_to_all | solution.py:540
  129.5 10.7 %collective-permute-start.3 = (bf16[256,128]{1,0:T(8,128)(2,1)S(1)}, bf16[256,128]{1,0:T(8,128)(2,1)S(1)}, u32[]{:S(2)}, u32[]{:S(2)}) collective-permute-start(bf16[256,128]{1,0:T(8,128)(2,1)S(1)} %get-tuple-element.25), channel_id=1, source_target_pairs={{0,3},{1,0},{2,1},{3,2},{4,7},{5,4},{6,5},{7,6},{8,11},{9,8},{10,9... | collective-permute-start | bytes 196616 | tf_op jit(solution)/shard_map/ppermute | solution.py:442
  131.6 8.6 %collective-permute-start.4 = (bf16[256,128]{1,0:T(8,128)(2,1)S(1)}, bf16[256,128]{1,0:T(8,128)(2,1)S(1)}, u32[]{:S(2)}, u32[]{:S(2)}) collective-permute-start(bf16[256,128]{1,0:T(8,128)(2,1)S(1)} %get-tuple-element.26), channel_id=1, source_target_pairs={{0,2},{1,3},{2,0},{3,1},{4,6},{5,7},{6,4},{7,5},{8,10},{9,11},{10,... | collective-permute-start | bytes 196616 | tf_op jit(solution)/shard_map/ppermute | solution.py:442
  136.9 6.2 %collective-permute-start.5 = (bf16[256,128]{1,0:T(8,128)(2,1)S(1)}, bf16[256,128]{1,0:T(8,128)(2,1)S(1)}, u32[]{:S(2)}, u32[]{:S(2)}) collective-permute-start(bf16[256,128]{1,0:T(8,128)(2,1)S(1)} %get-tuple-element.27), channel_id=1, source_target_pairs={{0,1},{1,2},{2,3},{3,0},{4,5},{5,6},{6,7},{7,4},{8,9},{9,10},{10,1... | collective-permute-start | bytes 196616 | tf_op jit(solution)/shard_map/ppermute | solution.py:442
